TPU v7x, 512 devices: a 4x2x32 block of a 4x8x32 slice. The times are simulated.
512 devices in a mesh: grp: 2 (over y), fs: 32 (over z), tp: 8 (over x, core).
Axes of the slice: x: 4, y: 2, z: 32, core: 2. Of those that a mesh axis runs over, the one named last changes fastest.
The devices are a block of a 4x8x32 slice.
Arguments:
- tokens: bfloat16 [65536, 2048], P(('grp', 'fs')), parts along dimension 0, may hold values from -6 to 6
- mixer_gain: float32 [2048], replicated, may hold values from 0.1 to 1.9
- outer_weight: float32 [2048, 2048], P('fs', 'tp'), may hold values from -0.125 to 0.125
- inner_weight: float32 [2048, 2048], P('fs', 'tp'), may hold values from -0.125 to 0.125
- value_weight: float32 [2048, 2048], P('fs', 'tp'), may hold values from -0.125 to 0.125
- filter_taps: float32 [3, 2048], P(None, 'tp'), may hold values from -3.5 to 3.5
- mixer_weight: float32 [2048, 2048], P('tp', 'fs'), may hold values from -0.125 to 0.125
- outer_scale: float32 [8, 256], P('tp', 'fs'), may hold values from 0.5 to 2
- inner_scale: float32 [8, 256], P('tp', 'fs'), may hold values from 0.5 to 2
- value_scale: float32 [8, 256], P('tp', 'fs'), may hold values from 0.5 to 2
- mixer_scale: float32 [1, 2048], P(None, 'fs'), may hold values from 0.5 to 2
Outputs:
- layer_out: bfloat16 [65536, 2048], P(('grp', 'fs', 'tp')), parts along dimension 0
There are 2 independent parts, one for each index of `grp`. A program takes and returns all parts, laid end to end along the dimension named above; an argument that names none is the same for every part. Nothing has to cross between parts.
All inputs are finite; a program needn't handle non-finite values.
Results may differ from a plain program's by a relative error of at most 0.014.
Values may be sent and summed in bfloat16 or wider, within the bound.
No kernel may reach another device: no remote copies, remote signals or barrier semaphores. Data moves between devices by JAX's collectives and lax.ppermute only.
A program may use at most 64 MiB of HBM per device.

v0:
```python
import jax
import jax.numpy as jnp
from jax import lax
from jax.sharding import PartitionSpec as P

EPS = 1e-06


def in_order(parts, dim):
    parts = jnp.moveaxis(parts, 0, dim)
    shape = parts.shape
    return parts.reshape(*shape[:dim], shape[dim] * shape[dim + 1], *shape[dim + 2 :])


def gather_packed(arrays, axis, dims):
    line = jnp.concatenate([a.reshape(-1) for a in arrays])
    lines, at, done = (lax.all_gather(line, axis), 0, [])
    for a, dim in zip(arrays, dims):
        parts = lines[:, at : at + a.size].reshape(-1, *a.shape)
        done.append(in_order(parts, dim))
        at += a.size
    return tuple(done)


def sent_together(arrays, axis, dim, along):
    ends, at = ([], 0)
    for a in arrays[:-1]:
        at += a.shape[along]
        ends.append(at)
    both = jnp.concatenate(arrays, axis=along)
    return tuple(jnp.split(lax.all_gather(both, axis, axis=dim, tiled=True), ends, axis=along))


def sent_to_all(array, axis):
    count = lax.axis_size(axis)
    return lax.all_to_all(
        jnp.broadcast_to(array[None], (count, *array.shape)), axis, 0, 0, tiled=True
    )


def collect(array, axis, dim):
    parts = sent_to_all(array, axis)
    return in_order(parts, dim)


def normed(rows, gain):
    values = rows.astype(jnp.float32)
    inverse = lax.rsqrt(jnp.mean(values * values, axis=-1, keepdims=True) + EPS)
    return (values * inverse * gain).astype(jnp.bfloat16)


def rounded(values):
    return lax.optimization_barrier(values.astype(jnp.bfloat16)).astype(jnp.float32)


def add_rows(left, piece):
    return jnp.dot(left, piece, preferred_element_type=jnp.float32)


def per_device(
    tokens,
    mixer_gain,
    outer_weight,
    inner_weight,
    value_weight,
    filter_taps,
    mixer_weight,
    outer_scale,
    inner_scale,
    value_scale,
    mixer_scale,
):
    gathered = gather_packed(
        (outer_scale, inner_scale, value_scale, mixer_scale), "fs", (1, 1, 1, 1)
    )
    outer_col, inner_col, value_col, mixer_col = [piece.reshape(-1) for piece in gathered]
    seq_rows = tokens.shape[0]
    normal_rows = normed(tokens, mixer_gain)

    def fold_one(piece):
        return add_rows(normal_rows, piece)

    pieces = sent_together(
        (
            outer_weight.astype(jnp.bfloat16),
            inner_weight.astype(jnp.bfloat16),
            value_weight.astype(jnp.bfloat16),
        ),
        "fs",
        0,
        1,
    )
    outer_sum = fold_one(pieces[0])
    inner_sum = fold_one(pieces[1])
    value_sum = fold_one(pieces[2])
    outer = rounded(outer_sum * outer_col)
    inner = rounded(inner_sum * inner_col)
    value = rounded(value_sum * value_col)
    padded = jnp.pad(inner * value, ((2, 0), (0, 0)))
    filtered = (
        filter_taps[0] * padded[0:seq_rows]
        + filter_taps[1] * padded[1 : seq_rows + 1]
        + filter_taps[2] * padded[2:]
    )
    gated = (outer * filtered).astype(jnp.bfloat16)
    mixer_full = collect(mixer_weight.astype(jnp.bfloat16), "fs", 1)
    return lax.psum_scatter(
        (jnp.dot(gated, mixer_full, preferred_element_type=jnp.float32) * mixer_col).astype(
            jnp.bfloat16
        ),
        "tp",
        scatter_dimension=0,
        tiled=True,
    )


def solution(mesh):
    in_specs = (
        P(("grp", "fs"), None),
        P(),
        P("fs", "tp"),
        P("fs", "tp"),
        P("fs", "tp"),
        P(None, "tp"),
        P("tp", "fs"),
        P("tp", "fs"),
        P("tp", "fs"),
        P("tp", "fs"),
        P(None, "fs"),
    )
    out_specs = P(("grp", "fs", "tp"), None)
    return jax.shard_map(
        per_device, mesh=mesh, in_specs=in_specs, out_specs=out_specs, check_vma=False
    )
```

profile of v0, /device:TPU:39, one launch (start us, length us, event | category | flops | bytes accessed | tf_op | source)
XLA Modules:
  0.0 329.1 jit_solution(2194338141352376970)
XLA Ops:
  6.5 0.0 copy-start.2
  6.5 0.9 convert_element_type.56
  7.4 1.1 broadcast_in_dim.2
  8.5 45.5 %all-to-all-start = ((bf16[32,256,64]{1,2,0:T(8,128)(2,1)}), bf16[32,256,64]{1,2,0:T(8,128)(2,1)S(1)}, u32[]{:S(2)}, u32[]{:S(2)}) async-start(bf16[32,256,64]{1,2,0:T(8,128)(2,1)} %broadcast_in_dim.2), calls=%async_computation | async-start | bytes 2097152 | tf_op jit(solution)/shard_map/all_to_all | solution.py:36
  54.0 0.1 all-gather.3.cloned.1.call-start
  54.1 0.8 convert_element_type.46
  54.9 0.8 convert_element_type.47
  55.8 0.8 convert_element_type.48
  56.6 0.6 pad_maximum_fusion
  57.3 0.1 all-gather.3.cloned.1.call-update
  57.3 0.1 reduce-scatter.2.cloned.1.call-start
  57.4 1.3 dynamic-slice
  59.4 0.9 maximum_dynamic-update-slice_fusion
  60.3 172.7 %all-reduce.1 = f32[2816]{0:T(1024)S(1)} all-reduce(f32[2816]{0:T(1024)S(1)} %maximum_dynamic-update-slice_fusion), channel_id=2, replica_groups=mesh['grp'=2,'fs'=32,'tp'=8] {'fs'}, use_global_device_ids=true, to_apply=%add.1 | all-reduce | flops 2816 | bytes 22528
  233.0 0.1 reshape.34
  233.1 0.1 slice.40
  233.2 0.1 mul.120
  233.2 0.1 fusion.16
  233.3 0.1 mul.100
  233.4 0.1 mul.108
  233.5 0.1 mul.105
  233.6 0.8 fusion.17
  234.4 3.1 fusion
  237.5 0.0 all-gather.3.cloned.1.call-done
  237.5 0.0 copy-done.2
  237.5 0.0 copy-start
  237.5 0.0 copy-start.1
  237.5 4.0 %fusion.4 = bf16[1024,256]{1,0:T(8,128)(2,1)S(1)} fusion(bf16[2048,768]{1,0:T(8,128)(2,1)} %all-gather.3.cloned.1.call-done, f32[256]{0:T(256)S(1)} %mul.105, bf16[1024,2048]{1,0:T(8,128)(2,1)} %param.11, f32[2048]{0:T(1024)S(1)} %copy-done.2, f32[1024]{0:T(1024)S(1)} %add_rsqrt_fusion), kind=kOutput, calls=%fused_computation.10 | convolution fusion | flops 1082654720 | bytes 5780480 | tf_op jit(solution)/shard_map/dot_general | solution.py:57
  241.5 0.0 copy-done
  241.5 0.8 copy-done.1
  242.3 1.4 fusion.3
  243.6 1.3 fusion.5
  245.0 0.1 convert_multiply_fusion.2
  245.1 0.0 all-to-all-done
  245.1 3.4 %multiply_convert_fusion = bf16[1024,2048]{1,0:T(8,128)(2,1)} fusion(bf16[256,2048]{0,1:T(8,128)(2,1)S(1)} %bitcast.12, f32[2048]{0:T(1024)S(1)} %mul.120, f32[1024,256]{1,0:T(8,128)S(1)} %convert_multiply_fusion.2, bf16[1024,256]{1,0:T(8,128)(2,1)S(1)} %fusion.3, f32[256]{0:T(256)S(1)} %bitcast.14, f32[256]{0:T(256)S(1)} %bitcast.15, f32[256]{0:T(256)S(1)} %bitcast.13), kind=kOutput, calls=%fused_computation.5 | convolution fusion | flops 1080033280 | bytes 6827008 | tf_op jit(solution)/shard_map/dot_general | solution.py:108
  248.6 0.1 reduce-scatter.2.cloned.1.call-update
  248.6 73.6 %reduce-scatter.2.cloned.1.call-done = bf16[128,2048]{1,0:T(8,128)(2,1)} async-done(((bf16[1024,2048]{1,0:T(8,128)(2,1)}), bf16[128,2048]{1,0:T(8,128)(2,1)}) %reduce-scatter.2.cloned.1.call-update) | async-done | bytes 524304 | tf_op jit(solution)/shard_map/reduce_scatter | solution.py:107
  (2 shorter events, 0.0 us)
Async XLA Ops:
  6.5 231.0 %copy-start.2 = (f32[2048]{0:T(1024)S(1)}, f32[2048]{0:T(1024)}, u32[]{:S(2)}) copy-start(f32[2048]{0:T(1024)} %param.12) | copy-start | bytes 24580
  8.5 236.6 %all-to-all-start = ((bf16[32,256,64]{1,2,0:T(8,128)(2,1)}), bf16[32,256,64]{1,2,0:T(8,128)(2,1)S(1)}, u32[]{:S(2)}, u32[]{:S(2)}) async-start(bf16[32,256,64]{1,2,0:T(8,128)(2,1)} %broadcast_in_dim.2), calls=%async_computation | async-start | bytes 2097152 | tf_op jit(solution)/shard_map/all_to_all | solution.py:36
  54.0 183.5 %all-gather.3.cloned.1.call-start = ((), (), s32[]{:S(2)}) async-start(), calls=%async_computation.2 | async-start | bytes 3244032 | tf_op jit(solution)/shard_map/all_gather | solution.py:31
  57.3 264.9 %reduce-scatter.2.cloned.1.call-start = ((), (), s32[]{:S(2)}) async-start(), calls=%async_computation.3 | async-start | bytes 4718592 | tf_op jit(solution)/shard_map/reduce_scatter | solution.py:107
  237.5 4.0 %copy-start = (bf16[1024,2048]{1,0:T(8,128)(2,1)S(1)}, bf16[1024,2048]{1,0:T(8,128)(2,1)}, u32[]{:S(2)}) copy-start(bf16[1024,2048]{1,0:T(8,128)(2,1)} %param.11) | copy-start | bytes 12582916
  237.5 4.7 %copy-start.1 = (bf16[2048,768]{1,0:T(8,128)(2,1)S(1)}, bf16[2048,768]{1,0:T(8,128)(2,1)}, u32[]{:S(2)}) copy-start(bf16[2048,768]{1,0:T(8,128)(2,1)} %all-gather.3.cloned.1.call-done) | copy-start | bytes 9437188
Sparse Core Ops, SparseCore 0:
  57.4 167.4 all-gather.2
  248.7 73.4 reduce-scatter.1
where the time goes:
time: 330 us; the launch traced here: 329 us
  blocking collectives  173 us (52%)
  waiting for transfers between devices  73.7 us (22%)
  starting transfers between devices  45.6 us (14%)
  between operations  14.2 us (4%)
  matrix products  10.1 us (3%)
  other arithmetic  8.13 us (2%)
  local copies, waits for them, and re-layouts  4.59 us (1%)
    unnamed x1, blocking collectives  173 us
    reduce_scatter x1, waiting for transfers between devices, per_device(): lax.psum_scatter((jnp.dot(gated, mixer_full, preferred_element_type=jnp.f...  73.6 us
    all_to_all x1, starting transfers between devices, sent_to_all(): lax.all_to_all(jnp.broadcast_to(array[None], (count, *array.shape)), axis...  45.5 us
    dot_general x3, matrix products, add_rows(): return jnp.dot(left, piece, preferred_element_type=jnp.float32)  6.65 us
  transfers between devices with their start and end apart: 3, of which 1 were waited for; matrix products, arithmetic and copies ran while one was open for 5% of the time, Pallas kernels for 0%

commit v1 on v0

v1 whole, which is shorter than its diff:
```python
import jax
import jax.numpy as jnp
from jax import lax
from jax.sharding import PartitionSpec as P

EPS = 1e-06
LIFT = 2.0**18
LOW = 2.0**12
LANES = 128


def normed(rows, gain):
    values = rows.astype(jnp.float32)
    inverse = lax.rsqrt(jnp.mean(values * values, axis=-1, keepdims=True) + EPS)
    return (values * inverse * gain).astype(jnp.bfloat16)


def rounded(values):
    return lax.optimization_barrier(values.astype(jnp.bfloat16)).astype(jnp.float32)


def lifted(weight):
    return (weight.astype(jnp.bfloat16).astype(jnp.float32) * LIFT).astype(jnp.float16)


def lane_blocks(array):
    return [array[:, at : at + LANES] for at in range(0, array.shape[1], LANES)]


def scale_rows(scales):
    flat = jnp.concatenate([s.reshape(-1) for s in scales])
    flat = jnp.pad(flat, (0, LANES - flat.size))
    high = flat.astype(jnp.float16)
    low = ((flat - high.astype(jnp.float32)) * LOW).astype(jnp.float16)
    return jnp.pad(jnp.stack([high, low]), ((0, 6), (0, 0)))


def gathered(weights, scales):
    rows = weights[0].shape[0]
    blocks = [b for w in weights for b in lane_blocks(lifted(w))]
    packed = jnp.concatenate(blocks + [scale_rows(scales)], axis=0)
    pieces = lax.all_gather(packed, "fs")
    count = pieces.shape[0]

    def block(at):
        return pieces[:, at * rows : (at + 1) * rows].reshape(count * rows, LANES)

    full, at = [], 0
    for w in weights:
        width = w.shape[1] // LANES
        both = jnp.concatenate([block(at + k) for k in range(width)], axis=1)
        full.append(both.astype(jnp.float32).astype(jnp.bfloat16))
        at += width
    top = pieces[:, at * rows].astype(jnp.float32) + pieces[:, at * rows + 1].astype(
        jnp.float32
    ) * (1.0 / LOW)
    columns, start = [], 0
    for s in scales:
        columns.append(top[:, start : start + s.size].reshape(-1) * (1.0 / LIFT))
        start += s.size
    return full, columns


def summed_rows(left, weight, scale):
    count = lax.axis_size("tp")
    chips = count // 2
    me = lax.axis_index("tp")
    chip, core = me // 2, me % 2
    rows = left.shape[0] // count
    width = left.shape[1]
    grid = left.reshape(chips, 2, rows, width)

    def mine(which):
        picked = lax.dynamic_slice_in_dim(grid, which, 1, 1).reshape(chips, rows, width)
        twice = jnp.concatenate([picked, picked], axis=0)
        return lax.dynamic_slice_in_dim(twice, chip, chips, 0).reshape(chips * rows, width)

    def part(these):
        return (
            lax.dot_general(
                these, weight, (((1,), (1,)), ((), ())), preferred_element_type=jnp.float32
            )
            * scale
        )

    swap = [(i, i ^ 1) for i in range(count)]
    theirs = lax.ppermute(part(mine(1 - core)).astype(jnp.bfloat16), "tp", swap)
    pair = part(mine(core)).astype(jnp.bfloat16).astype(jnp.float32) + theirs.astype(jnp.float32)
    total = pair[:rows]
    for step in range(1, chips):
        move = [(i, (i + 2 * step) % count) for i in range(count)]
        sent = pair[step * rows : (step + 1) * rows].astype(jnp.bfloat16)
        total = total + lax.ppermute(sent, "tp", move).astype(jnp.float32)
    return total.astype(jnp.bfloat16)


def per_device(
    tokens,
    mixer_gain,
    outer_weight,
    inner_weight,
    value_weight,
    filter_taps,
    mixer_weight,
    outer_scale,
    inner_scale,
    value_scale,
    mixer_scale,
):
    seq_rows = tokens.shape[0]
    full, columns = gathered(
        (outer_weight, inner_weight, value_weight, mixer_weight.T),
        (outer_scale, inner_scale, value_scale, mixer_scale),
    )
    normal_rows = normed(tokens, mixer_gain)
    outer, inner, value = [
        rounded(jnp.dot(normal_rows, w, preferred_element_type=jnp.float32) * c)
        for w, c in zip(full[:3], columns[:3])
    ]
    padded = jnp.pad(inner * value, ((2, 0), (0, 0)))
    filtered = (
        filter_taps[0] * padded[0:seq_rows]
        + filter_taps[1] * padded[1 : seq_rows + 1]
        + filter_taps[2] * padded[2:]
    )
    gated = (outer * filtered).astype(jnp.bfloat16)
    return summed_rows(gated, full[3], columns[3])


def solution(mesh):
    in_specs = (
        P(("grp", "fs"), None),
        P(),
        P("fs", "tp"),
        P("fs", "tp"),
        P("fs", "tp"),
        P(None, "tp"),
        P("tp", "fs"),
        P("tp", "fs"),
        P("tp", "fs"),
        P("tp", "fs"),
        P(None, "fs"),
    )
    out_specs = P(("grp", "fs", "tp"), None)
    return jax.shard_map(
        per_device, mesh=mesh, in_specs=in_specs, out_specs=out_specs, check_vma=False
    )
```

time: 330 us -> 190 us (0.58)
  blocking collectives: 173 us -> 111 us
  waiting for transfers between devices: 73.7 us -> 24.3 us
  starting transfers between devices: 45.6 us -> 24.1 us
  between operations: 14.2 us -> 0.2 us
  matrix products: 10.1 us -> 15 us
    unnamed x1 -> x0, blocking collectives: 173 us -> none
    all_gather x0 -> x1, blocking collectives: none -> 111 us  [gathered(): pieces = lax.all_gather(packed, 'fs')]
    reduce_scatter x1 -> x0, waiting for transfers between devices: 73.6 us -> none  [per_device(): lax.psum_scatter((jnp.dot(gated, mixer_full, preferred_element_type=jnp.f...]
    all_to_all x1 -> x0, starting transfers between devices: 45.5 us -> none  [sent_to_all(): lax.all_to_all(jnp.broadcast_to(array[None], (count, *array.shape)), axis...]
    ppermute x0 -> x4, waiting for transfers between devices: none -> 24.3 us  [the longest x3 20.7 us: summed_rows(): total = total + lax.ppermute(sent, 'tp', move).astype(jnp.float32)]
    ppermute x0 -> x4, starting transfers between devices: none -> 24.1 us  [the longest x1 16 us: summed_rows(): theirs = lax.ppermute(part(mine(1 - core)).astype(jnp.bfloat16), 'tp', swap)]
    dot_general x4 -> x5, matrix products: 10.1 us -> 15 us  [the longest x3 13.4 us: per_device(): jnp.dot(normal_rows, w, preferred_element_type=jnp.float32) * c]
  transfers between devices with their start and end apart: 3 -> 4, of which waited for: 1 -> 4; matrix products, arithmetic and copies ran while one was open for 5% -> 0% of each run, Pallas kernels for 0% -> 0%
where the time goes in v1:
time: 190 us; the launch traced here: 187 us
  blocking collectives  111 us (58%)
  waiting for transfers between devices  24.3 us (13%)
  starting transfers between devices  24.1 us (13%)
  matrix products  15 us (8%)
  other arithmetic  10.3 us (5%)
  local copies, waits for them, and re-layouts  2.81 us (1%)
    all_gather x1, blocking collectives, gathered(): pieces = lax.all_gather(packed, 'fs')  111 us
    ppermute x3, waiting for transfers between devices, summed_rows(): total = total + lax.ppermute(sent, 'tp', move).astype(jnp.float32)  20.7 us
    ppermute x1, starting transfers between devices, summed_rows(): theirs = lax.ppermute(part(mine(1 - core)).astype(jnp.bfloat16), 'tp', swap)  16 us
    dot_general x3, matrix products, per_device(): jnp.dot(normal_rows, w, preferred_element_type=jnp.float32) * c  13.4 us
    ppermute x3, starting transfers between devices, summed_rows(): total = total + lax.ppermute(sent, 'tp', move).astype(jnp.float32)  8.15 us
  transfers between devices with their start and end apart: 4, of which 4 were waited for; matrix products, arithmetic and copies ran while one was open for 0% of the time, Pallas kernels for 0%

profile of v1, /device:TPU:39, one launch (start us, length us, event | category | flops | bytes accessed | tf_op | source)
XLA Modules:
  0.0 187.4 jit_solution(16668316900437748541)
XLA Ops:
  0.0 0.8 convert_bitcast_fusion.1
  0.8 0.9 multiply_convert_fusion.6
  1.6 0.8 multiply_convert_fusion.5
  2.5 0.8 multiply_convert_fusion.4
  3.3 0.8 fusion.20
  4.3 110.6 %all-gather.2 = f16[16640,128]{1,0:T(8,128)(2,1)S(1)} all-gather(f16[520,128]{1,0:T(8,128)(2,1)S(1)} %constant_dynamic-update-slice_fusion), channel_id=2, replica_groups=mesh['grp'=2,'fs'=32,'tp'=8] {'fs'}, dimensions={0}, use_global_device_ids=true | all-gather | bytes 4392960 | tf_op jit(solution)/shard_map/all_gather | solution.py:42
  115.0 0.0 copy-start.2
  115.0 2.2 %fusion.32 = (f16[32,64,128]{2,1,0:T(8,128)(2,1)S(1)}, f16[32,64,128]{2,1,0:T(8,128)(2,1)S(1)}, f16[32,64,128]{2,1,0:T(8,128)(2,1)S(1)}, f16[32,64,128]{2,1,0:T(...) fusion(f16[32,520,128]{2,1,0:T(8,128)(2,1)S(1)} %bitcast.34), kind=kLoop, calls=%fused_computation.77 | loop fusion | bytes 8388608 | tf_op jit(solution)/shard_map/slice | solution.py:46
  117.2 0.0 copy-start.3
  117.2 0.1 slice_multiply_fusion
  117.3 0.1 slice_multiply_fusion.3
  117.3 0.0 copy-done.2
  117.4 3.1 %fusion = f32[1024]{0:T(1024)S(1)} fusion(bf16[1024,2048]{1,0:T(8,128)(2,1)} %param.11), kind=kLoop, calls=%fused_computation.2 | loop fusion | flops 6290432 | bytes 4198400 | tf_op jit(solution)/shard_map/reduce_sum | solution.py:14
  120.4 0.1 mul.200
  120.5 0.1 mul.176
  120.6 0.0 copy-done.3
  120.6 4.6 %fusion.3 = bf16[1024,256]{1,0:T(8,128)(2,1)} fusion(f16[2048,128]{1,0:T(8,128)(2,1)} %bitcast.45, f16[2048,128]{1,0:T(8,128)(2,1)} %bitcast.46, f32[256]{0:T(256)S(1)} %mul.176, bf16[1024,2048]{1,0:T(8,128)(2,1)} %param.11, f32[2048]{0:T(1024)S(1)} %copy-done.3, f32[1024]{0:T(1024)S(1)} %add_rsqrt_fusion), kind=kOutput, calls=%fused_computation.15 | convolution fusion | flops 1084227584 | bytes 5780480 | tf_op jit(solution)/shard_map/dot_general | solution.py:117
  125.2 0.1 mul.186
  125.3 4.3 %fusion.5 = bf16[1024,256]{1,0:T(8,128)(2,1)} fusion(f16[2048,128]{1,0:T(8,128)(2,1)S(1)} %bitcast.43, f16[2048,128]{1,0:T(8,128)(2,1)S(1)} %bitcast.44, f32[256]{0:T(256)S(1)} %mul.186, bf16[1024,2048]{1,0:T(8,128)(2,1)} %param.11, f32[2048]{0:T(1024)S(1)} %copy-done.3, f32[1024]{0:T(1024)S(1)} %add_rsqrt_fusion), kind=kOutput, calls=%fused_computation.17 | convolution fusion | flops 1084227584 | bytes 5780480 | tf_op jit(solution)/shard_map/dot_general | solution.py:117
  129.6 0.1 mul.182
  129.7 0.0 copy-start.1
  129.7 0.0 copy-start
  129.8 4.4 %fusion.4 = bf16[1024,256]{1,0:T(8,128)(2,1)} fusion(f16[2048,128]{1,0:T(8,128)(2,1)S(1)} %bitcast.41, f16[2048,128]{1,0:T(8,128)(2,1)S(1)} %bitcast.42, f32[256]{0:T(256)S(1)} %mul.182, bf16[1024,2048]{1,0:T(8,128)(2,1)} %param.11, f32[2048]{0:T(1024)S(1)} %copy-done.3, f32[1024]{0:T(1024)S(1)} %add_rsqrt_fusion), kind=kOutput, calls=%fused_computation.16 | convolution fusion | flops 1084227584 | bytes 5780480 | tf_op jit(solution)/shard_map/dot_general | solution.py:117
  134.2 0.0 copy-done.1
  134.2 1.1 convert_multiply_fusion.2
  135.3 0.0 copy-done
  135.3 0.4 multiply_convert_fusion.2
  135.8 0.1 fusion.18
  135.9 0.8 multiply_convert_fusion
  136.7 16.0 %collective-permute-start = (bf16[512,2048]{1,0:T(8,128)(2,1)S(1)}, bf16[512,2048]{1,0:T(8,128)(2,1)S(1)}, u32[]{:S(2)}, u32[]{:S(2)}) collective-permute-start(bf16[512,2048]{1,0:T(8,128)(2,1)S(1)} %multiply_convert_fusion), channel_id=1, source_target_pairs={{0,1},{1,0},{2,3},{3,2},{4,5},{5,4},{6,7},{7,6},{8,9},{9,8},{10,11... | collective-permute-start | bytes 6291464 | tf_op jit(solution)/shard_map/ppermute | solution.py:87
  152.7 0.1 fusion.19
  152.8 3.6 %collective-permute-done = bf16[512,2048]{1,0:T(8,128)(2,1)S(1)} collective-permute-done((bf16[512,2048]{1,0:T(8,128)(2,1)S(1)}, bf16[512,2048]{1,0:T(8,128)(2,1)S(1)}, u32[]{:S(2)}, u32[]{:S(2)}) %collective-permute-start) | collective-permute-done | bytes 2097184 | tf_op jit(solution)/shard_map/ppermute | solution.py:87
  156.4 0.9 fusion.36
  157.3 0.1 fusion.34
  157.4 2.0 %collective-permute-start.1 = (bf16[128,2048]{1,0:T(8,128)(2,1)S(1)}, bf16[128,2048]{1,0:T(8,128)(2,1)S(1)}, u32[]{:S(2)}, u32[]{:S(2)}) collective-permute-start(bf16[128,2048]{1,0:T(8,128)(2,1)S(1)} %get-tuple-element.17), channel_id=1, source_target_pairs={{0,2},{1,3},{2,4},{3,5},{4,6},{5,7},{6,0},{7,1},{8,10},{9,11},{10,... | collective-permute-start | bytes 1572872 | tf_op jit(solution)/shard_map/ppermute | solution.py:93
  159.4 3.4 %collective-permute-start.3 = (bf16[128,2048]{1,0:T(8,128)(2,1)S(1)}, bf16[128,2048]{1,0:T(8,128)(2,1)S(1)}, u32[]{:S(2)}, u32[]{:S(2)}) collective-permute-start(bf16[128,2048]{1,0:T(8,128)(2,1)S(1)} %get-tuple-element.18), channel_id=1, source_target_pairs={{0,6},{1,7},{2,0},{3,1},{4,2},{5,3},{6,4},{7,5},{8,14},{9,15},{10,... | collective-permute-start | bytes 1572872 | tf_op jit(solution)/shard_map/ppermute | solution.py:93
  162.8 2.8 %collective-permute-start.2 = (bf16[128,2048]{1,0:T(8,128)(2,1)S(1)}, bf16[128,2048]{1,0:T(8,128)(2,1)S(1)}, u32[]{:S(2)}, u32[]{:S(2)}) collective-permute-start(bf16[128,2048]{1,0:T(8,128)(2,1)S(1)} %get-tuple-element.19), channel_id=1, source_target_pairs={{0,4},{1,5},{2,6},{3,7},{4,0},{5,1},{6,2},{7,3},{8,12},{9,13},{10,... | collective-permute-start | bytes 1572872 | tf_op jit(solution)/shard_map/ppermute | solution.py:93
  165.6 6.9 %collective-permute-done.1 = bf16[128,2048]{1,0:T(8,128)(2,1)S(1)} collective-permute-done((bf16[128,2048]{1,0:T(8,128)(2,1)S(1)}, bf16[128,2048]{1,0:T(8,128)(2,1)S(1)}, u32[]{:S(2)}, u32[]{:S(2)}) %collective-permute-start.1) | collective-permute-done | bytes 524320 | tf_op jit(solution)/shard_map/ppermute | solution.py:93
  172.5 3.6 %collective-permute-done.3 = bf16[128,2048]{1,0:T(8,128)(2,1)S(1)} collective-permute-done((bf16[128,2048]{1,0:T(8,128)(2,1)S(1)}, bf16[128,2048]{1,0:T(8,128)(2,1)S(1)}, u32[]{:S(2)}, u32[]{:S(2)}) %collective-permute-start.3) | collective-permute-done | bytes 524320 | tf_op jit(solution)/shard_map/ppermute | solution.py:93
  176.1 10.2 %collective-permute-done.2 = bf16[128,2048]{1,0:T(8,128)(2,1)S(1)} collective-permute-done((bf16[128,2048]{1,0:T(8,128)(2,1)S(1)}, bf16[128,2048]{1,0:T(8,128)(2,1)S(1)}, u32[]{:S(2)}, u32[]{:S(2)}) %collective-permute-start.2) | collective-permute-done | bytes 524320 | tf_op jit(solution)/shard_map/ppermute | solution.py:93
  186.3 1.1 fusion.8
  (15 shorter events, 0.2 us)
Async XLA Ops:
  115.0 2.3 %copy-start.2 = (f32[3,256]{1,0:T(4,128)S(1)}, f32[3,256]{1,0:T(4,128)}, u32[]{:S(2)}) copy-start(f32[3,256]{1,0:T(4,128)} %param.16) | copy-start | bytes 9220
  117.2 3.4 %copy-start.3 = (f32[2048]{0:T(1024)S(1)}, f32[2048]{0:T(1024)}, u32[]{:S(2)}) copy-start(f32[2048]{0:T(1024)} %param.12) | copy-start | bytes 24580
  129.7 4.4 %copy-start.1 = (bf16[1024,256]{1,0:T(8,128)(2,1)S(1)}, bf16[1024,256]{1,0:T(8,128)(2,1)}, u32[]{:S(2)}) copy-start(bf16[1024,256]{1,0:T(8,128)(2,1)} %fusion.5) | copy-start | bytes 1572868
  129.7 5.6 %copy-start = (bf16[1024,256]{1,0:T(8,128)(2,1)S(1)}, bf16[1024,256]{1,0:T(8,128)(2,1)}, u32[]{:S(2)}) copy-start(bf16[1024,256]{1,0:T(8,128)(2,1)} %fusion.3) | copy-start | bytes 1572868
  136.7 19.8 %collective-permute-start = (bf16[512,2048]{1,0:T(8,128)(2,1)S(1)}, bf16[512,2048]{1,0:T(8,128)(2,1)S(1)}, u32[]{:S(2)}, u32[]{:S(2)}) collective-permute-start(bf16[512,2048]{1,0:T(8,128)(2,1)S(1)} %multiply_convert_fusion), channel_id=1, source_target_pairs={{0,1},{1,0},{2,3},{3,2},{4,5},{5,4},{6,7},{7,6},{8,9},{9,8},{10,11... | collective-permute-start | bytes 6291464 | tf_op jit(solution)/shard_map/ppermute | solution.py:87
  157.4 15.0 %collective-permute-start.1 = (bf16[128,2048]{1,0:T(8,128)(2,1)S(1)}, bf16[128,2048]{1,0:T(8,128)(2,1)S(1)}, u32[]{:S(2)}, u32[]{:S(2)}) collective-permute-start(bf16[128,2048]{1,0:T(8,128)(2,1)S(1)} %get-tuple-element.17), channel_id=1, source_target_pairs={{0,2},{1,3},{2,4},{3,5},{4,6},{5,7},{6,0},{7,1},{8,10},{9,11},{10,... | collective-permute-start | bytes 1572872 | tf_op jit(solution)/shard_map/ppermute | solution.py:93
  159.4 16.7 %collective-permute-start.3 = (bf16[128,2048]{1,0:T(8,128)(2,1)S(1)}, bf16[128,2048]{1,0:T(8,128)(2,1)S(1)}, u32[]{:S(2)}, u32[]{:S(2)}) collective-permute-start(bf16[128,2048]{1,0:T(8,128)(2,1)S(1)} %get-tuple-element.18), channel_id=1, source_target_pairs={{0,6},{1,7},{2,0},{3,1},{4,2},{5,3},{6,4},{7,5},{8,14},{9,15},{10,... | collective-permute-start | bytes 1572872 | tf_op jit(solution)/shard_map/ppermute | solution.py:93
  162.8 23.5 %collective-permute-start.2 = (bf16[128,2048]{1,0:T(8,128)(2,1)S(1)}, bf16[128,2048]{1,0:T(8,128)(2,1)S(1)}, u32[]{:S(2)}, u32[]{:S(2)}) collective-permute-start(bf16[128,2048]{1,0:T(8,128)(2,1)S(1)} %get-tuple-element.19), channel_id=1, source_target_pairs={{0,4},{1,5},{2,6},{3,7},{4,0},{5,1},{6,2},{7,3},{8,12},{9,13},{10,... | collective-permute-start | bytes 1572872 | tf_op jit(solution)/shard_map/ppermute | solution.py:93

commit v2 on v1

v2 whole, which is shorter than its diff:
```python
import jax
import jax.numpy as jnp
from jax import lax
from jax.experimental import pallas as pl
from jax.experimental.pallas import tpu as pltpu
from jax.sharding import PartitionSpec as P

EPS = 1e-06
LIFT = 2.0**18
LOW = 2.0**12
LANES = 128
ROWS = 256
VMEM_BYTES = 28 * 2**20


def pack_kernel(*refs):
    *arrays, out = refs
    weights, scales = arrays[:4], arrays[4:]
    at = 0
    for w in weights:
        rows, width = w.shape
        for k in range(0, width, LANES):
            block = w[:, k : k + LANES].astype(jnp.bfloat16).astype(jnp.float32)
            out[at : at + rows, :] = block * LIFT
            at += rows
    out[at:, :] = jnp.zeros((out.shape[0] - at, LANES), jnp.float32)
    start = 0
    for s in scales:
        value, stop = s[...], start + s.shape[1]
        high = value.astype(jnp.bfloat16).astype(jnp.float32)
        rest = (value - high) * LOW
        middle = rest.astype(jnp.bfloat16).astype(jnp.float32)
        for k, term in enumerate((high, middle, rest - middle)):
            out[at + k : at + k + 1, start:stop] = term
        start = stop


def gathered(weights, scales):
    rows = weights[0].shape[0]
    total = sum(w.shape[1] for w in weights) // LANES * rows + 8
    packed = pl.pallas_call(
        pack_kernel,
        out_shape=jax.ShapeDtypeStruct((total, LANES), jnp.float32),
        compiler_params=pltpu.CompilerParams(vmem_limit_bytes=4 * 2**20),
    )(*weights, *scales)
    pieces = lax.all_gather(packed.astype(jnp.float16), "fs")
    blocks = pieces.shape[1] // rows
    terms = [pieces[:, blocks * rows + k].astype(jnp.float32) for k in range(3)]
    top = terms[0] + (terms[1] + terms[2]) * (1.0 / LOW)
    columns, start = [], 0
    for s in scales:
        columns.append(top[:, start : start + s.size].reshape(-1) * (1.0 / LIFT))
        start += s.size
    pieces = lax.optimization_barrier(pieces.astype(jnp.float32).astype(jnp.bfloat16))
    pieces = pltpu.with_memory_space_constraint(pieces, pltpu.VMEM)
    return pieces, (jnp.concatenate(columns[:-1]), columns[-1])


def summed_rows(left, weight, scale):
    count = lax.axis_size("tp")
    chips = count // 2
    core = lax.axis_index("tp") % 2
    rows = left.shape[0] // count
    grid = left.reshape(chips, 2, rows, left.shape[1])

    def part(which):
        these = lax.dynamic_slice_in_dim(grid, which, 1, 1).reshape(chips * rows, -1)
        return (
            lax.dot_general(
                these, weight, (((1,), (1,)), ((), ())), preferred_element_type=jnp.float32
            )
            * scale
        ).astype(jnp.bfloat16)

    swap = [(i, i ^ 1) for i in range(count)]
    theirs = lax.ppermute(part(1 - core), "tp", swap)
    pair = (part(core).astype(jnp.float32) + theirs.astype(jnp.float32)).astype(jnp.bfloat16)
    same_core = [list(range(which, count, 2)) for which in range(2)]
    parts = lax.all_to_all(
        pair.reshape(chips, rows, -1), "tp", 0, 0, axis_index_groups=same_core
    )
    total = parts[0].astype(jnp.float32)
    for k in range(1, chips):
        total = total + parts[k].astype(jnp.float32)
    return total.astype(jnp.bfloat16)


def gate_kernel(tokens, gain, pieces, columns, taps, out, mixer, weight, carry):
    @pl.when(pl.program_id(0) == 0)
    def _():
        carry[...] = jnp.zeros_like(carry)
        depth = weight.shape[0]
        rows = depth // pieces.shape[0]
        inputs = weight.shape[1] // LANES
        for k in range(inputs + mixer.shape[1] // LANES):
            full = pieces[:, k * rows : (k + 1) * rows, :]
            to, at = (weight, k) if k < inputs else (mixer, k - inputs)
            to[:, at * LANES : (at + 1) * LANES] = full.reshape(depth, LANES)

    values = tokens[...].astype(jnp.float32)
    inverse = lax.rsqrt(jnp.mean(values * values, axis=-1, keepdims=True) + EPS)
    normal = (values * inverse * gain[...]).astype(jnp.bfloat16)
    width = out.shape[1]

    def projected(at):
        cols = slice(at * width, (at + 1) * width)
        total = jnp.dot(normal, weight[:, cols], preferred_element_type=jnp.float32)
        return (total * columns[:, cols]).astype(jnp.bfloat16).astype(jnp.float32)

    product = projected(1) * projected(2)
    last = carry[...]
    carry[...] = product[-8:]
    row = lax.broadcasted_iota(jnp.int32, (8, width), 0)

    def shifted(by):
        moved = pltpu.roll(product, by, 0)
        head = jnp.where(row < by, pltpu.roll(last, by, 0), moved[:8])
        return jnp.concatenate([head, moved[8:]], axis=0)

    filtered = taps[0:1] * shifted(2) + taps[1:2] * shifted(1) + taps[2:3] * product
    out[...] = (projected(0) * filtered).astype(jnp.bfloat16)


def gated_rows(tokens, gain, pieces, columns, taps):
    rows, depth = tokens.shape
    width = taps.shape[1]
    whole = pl.BlockSpec(memory_space=pltpu.VMEM)
    return pl.pallas_call(
        gate_kernel,
        grid=(rows // ROWS,),
        in_specs=[pl.BlockSpec((ROWS, depth), lambda i: (i, 0)), whole, whole, whole, whole],
        out_specs=[pl.BlockSpec((ROWS, width), lambda i: (i, 0)), whole],
        out_shape=[
            jax.ShapeDtypeStruct((rows, width), jnp.bfloat16),
            jax.ShapeDtypeStruct((depth, width), jnp.bfloat16),
        ],
        scratch_shapes=[
            pltpu.VMEM((depth, 3 * width), jnp.bfloat16),
            pltpu.VMEM((8, width), jnp.float32),
        ],
        compiler_params=pltpu.CompilerParams(
            dimension_semantics=("arbitrary",), vmem_limit_bytes=VMEM_BYTES
        ),
    )(pltpu.with_memory_space_constraint(tokens, pltpu.HBM), gain.reshape(1, -1), pieces, columns.reshape(1, -1), taps)


def per_device(
    tokens,
    mixer_gain,
    outer_weight,
    inner_weight,
    value_weight,
    filter_taps,
    mixer_weight,
    outer_scale,
    inner_scale,
    value_scale,
    mixer_scale,
):
    pieces, columns = gathered(
        (outer_weight, inner_weight, value_weight, mixer_weight.T),
        (outer_scale, inner_scale, value_scale, mixer_scale),
    )
    gated, mixer_full = gated_rows(tokens, mixer_gain, pieces, columns[0], filter_taps)
    return summed_rows(gated, mixer_full, columns[1])


def solution(mesh):
    in_specs = (
        P(("grp", "fs"), None),
        P(),
        P("fs", "tp"),
        P("fs", "tp"),
        P("fs", "tp"),
        P(None, "tp"),
        P("tp", "fs"),
        P("tp", "fs"),
        P("tp", "fs"),
        P("tp", "fs"),
        P(None, "fs"),
    )
    out_specs = P(("grp", "fs", "tp"), None)
    return jax.shard_map(
        per_device, mesh=mesh, in_specs=in_specs, out_specs=out_specs, check_vma=False
    )
```

time: 190 us -> 183 us (0.963)
  blocking collectives: 111 us -> 138 us
  waiting for transfers between devices: 24.3 us -> 3.76 us
  matrix products: 15 us -> 1.51 us
  starting transfers between devices: 24.1 us -> 16 us
  Pallas kernels: 0 us -> 7.36 us
  other arithmetic: 10.3 us -> 4.05 us
  local copies, waits for them, and re-layouts: 2.81 us -> 8.58 us
    all_to_all x0 -> x1, blocking collectives: none -> 27.6 us  [summed_rows(): lax.all_to_all(pair.reshape(chips, rows, -1), 'tp', 0, 0, axis_index_grou...]
    ppermute x4 -> x1, waiting for transfers between devices: 24.3 us -> 3.76 us  [summed_rows(): theirs = lax.ppermute(part(1 - core), 'tp', swap)]
    dot_general x3 -> x0, matrix products: 13.4 us -> none  [per_device(): jnp.dot(normal_rows, w, preferred_element_type=jnp.float32) * c]
    ppermute x4 -> x1, starting transfers between devices: 24.1 us -> 16 us  [summed_rows(): theirs = lax.ppermute(part(1 - core), 'tp', swap)]
    unnamed x16 -> x22, local copies, waits for them, and re-layouts: 0.12 us -> 8.19 us
    pallas_call x0 -> x2, Pallas kernels: none -> 7.36 us  [the longest x1 7.27 us: gated_rows(): pl.pallas_call(gate_kernel, grid=(rows // ROWS,), in_specs=[pl.BlockSpec(...]
    reduce_sum x1 -> x0, other arithmetic: 3.07 us -> none  [normed(): inverse = lax.rsqrt(jnp.mean(values * values, axis=-1, keepdims=True) + EPS)]
    slice x4 -> x0, local copies, waits for them, and re-layouts: 2.31 us -> none  [the longest x1 2.17 us: block(): return pieces[:, at * rows:(at + 1) * rows].reshape(count * rows, LANES)]
  transfers between devices with their start and end apart: 4 -> 1, of which waited for: 4 -> 1; matrix products, arithmetic and copies ran while one was open for 0% -> 0% of each run, Pallas kernels for 0% -> 0%
where the time goes in v2:
time: 183 us; the launch traced here: 180 us
  blocking collectives  138 us (75%)
  starting transfers between devices  16 us (9%)
  local copies, waits for them, and re-layouts  8.58 us (5%)
  Pallas kernels  7.36 us (4%)
  other arithmetic  4.05 us (2%)
  waiting for transfers between devices  3.76 us (2%)
    all_gather x1, blocking collectives, gathered(): pieces = lax.all_gather(packed.astype(jnp.float16), 'fs')  111 us
    all_to_all x1, blocking collectives, summed_rows(): lax.all_to_all(pair.reshape(chips, rows, -1), 'tp', 0, 0, axis_index_grou...  27.6 us
    ppermute x1, starting transfers between devices, summed_rows(): theirs = lax.ppermute(part(1 - core), 'tp', swap)  16 us
    unnamed x22, local copies, waits for them, and re-layouts  8.19 us
    pallas_call x1, Pallas kernels, gated_rows(): pl.pallas_call(gate_kernel, grid=(rows // ROWS,), in_specs=[pl.BlockSpec(...  7.27 us
    ppermute x1, waiting for transfers between devices, summed_rows(): theirs = lax.ppermute(part(1 - core), 'tp', swap)  3.76 us
  transfers between devices with their start and end apart: 1, of which 1 were waited for; matrix products, arithmetic and copies ran while one was open for 0% of the time, Pallas kernels for 0%

profile of v2, /device:TPU:39, one launch (start us, length us, event | category | flops | bytes accessed | tf_op | source)
XLA Modules:
  0.0 179.5 jit_solution(14414159427537628405)
XLA Ops:
  0.0 0.0 copy-start.1
  0.0 0.8 copy-done.1
  0.8 0.0 copy-start.2
  0.8 0.8 copy-done.2
  1.7 0.0 copy-start.3
  1.7 0.8 copy-done.3
  2.5 0.0 copy-start.4
  2.5 0.8 copy-done.4
  3.4 0.0 copy-start.7
  3.4 0.7 copy-done.7
  4.0 0.0 copy-start.8
  4.0 0.7 copy-done.8
  4.7 0.0 copy-start.9
  4.7 0.7 copy-done.9
  5.3 0.0 copy-start.10
  5.3 0.7 copy-done.10
  6.0 0.1 shard_map.109
  6.1 110.6 %all-gather.2 = f16[16640,128]{1,0:T(8,128)(2,1)S(1)} all-gather(f16[520,128]{1,0:T(8,128)(2,1)S(1)} %convert_element_type.53), channel_id=2, replica_groups=mesh['grp'=2,'fs'=32,'tp'=8] {'fs'}, dimensions={0}, use_global_device_ids=true | all-gather | bytes 4392960 | tf_op jit(solution)/shard_map/all_gather | solution.py:46
  116.7 0.0 copy-start.5
  116.7 0.0 copy-start.6
  116.7 2.7 %convert_convert_fusion.pieces = bf16[32,520,128]{2,1,0:T(8,128)(2,1)} fusion(f16[32,520,128]{2,1,0:T(8,128)(2,1)S(1)} %bitcast.17), kind=kLoop, calls=%fused_computation | loop fusion | flops 4259840 | bytes 8519680 | tf_op jit(solution)/shard_map/convert_element_type | solution.py:54
  119.5 0.1 slice_multiply_fusion.3
  119.5 0.1 slice_multiply_fusion
  119.6 0.1 mul.59
  119.7 0.1 mul.57
  119.8 0.1 mul.55
  119.9 0.1 mul.62
  120.0 0.0 copy-done.5
  120.0 0.0 copy-done.6
  120.0 0.0 copy-start
  120.0 2.2 %copy-done = bf16[32,520,128]{2,1,0:T(8,128)(2,1)S(1)} copy-done((bf16[32,520,128]{2,1,0:T(8,128)(2,1)S(1)}, bf16[32,520,128]{2,1,0:T(8,128)(2,1)}, u32[]{:S(2)}) %copy-start) | copy-done | bytes 4259864
  122.2 7.3 %shard_map.110 = (bf16[1024,256]{1,0:T(8,128)(2,1)S(1)}, bf16[2048,256]{1,0:T(8,128)(2,1)S(1)}) custom-call(bf16[1024,2048]{1,0:T(8,128)(2,1)} %tokens.1, f32[1,2048]{1,0:T(1,128)S(1)} %bitcast.16, bf16[32,520,128]{2,1,0:T(8,128)(2,1)S(1)} %copy-done, f32[1,768]{1,0:T(1,128)S(1)} %reshape.51.columns, f32[3,256]{1,0:T(4,128)S(1)} %copy-done.6), custom_call_target="tpu_custom_call" | custom-call | tf_op jit(solution)/shard_map/pallas_call | solution.py:128
  129.5 0.7 multiply_convert_fusion
  130.3 16.0 %collective-permute-start = (bf16[512,2048]{1,0:T(8,128)(2,1)S(1)}, bf16[512,2048]{1,0:T(8,128)(2,1)S(1)}, u32[]{:S(2)}, u32[]{:S(2)}) collective-permute-start(bf16[512,2048]{1,0:T(8,128)(2,1)S(1)} %multiply_convert_fusion), channel_id=1, source_target_pairs={{0,1},{1,0},{2,3},{3,2},{4,5},{5,4},{6,7},{7,6},{8,9},{9,8},{10,11... | collective-permute-start | bytes 6291464 | tf_op jit(solution)/shard_map/ppermute | solution.py:76
  146.3 3.8 %collective-permute-done = bf16[512,2048]{1,0:T(8,128)(2,1)S(1)} collective-permute-done((bf16[512,2048]{1,0:T(8,128)(2,1)S(1)}, bf16[512,2048]{1,0:T(8,128)(2,1)S(1)}, u32[]{:S(2)}, u32[]{:S(2)}) %collective-permute-start) | collective-permute-done | bytes 2097184 | tf_op jit(solution)/shard_map/ppermute | solution.py:76
  150.1 0.8 add_convert_fusion
  150.8 27.6 %all_to_all.5 = bf16[4,128,2048]{2,1,0:T(8,128)(2,1)S(1)} all-to-all(bf16[4,128,2048]{2,1,0:T(8,128)(2,1)S(1)} %bitcast.19), channel_id=1, replica_groups={{0,2,4,6},{1,3,5,7},{8,10,12,14},{9,11,13,15},{16,18,20,22},{17,19,21,2..., dimensions={0} | all-to-all | bytes 4194304 | tf_op jit(solution)/shard_map/all_to_all | solution.py:79
  178.4 1.1 fusion
  (5 shorter events, 0.1 us)
Async XLA Ops:
  0.0 0.8 copy-start.1
  0.8 0.8 copy-start.2
  1.7 0.8 copy-start.3
  2.5 0.8 copy-start.4
  3.4 0.7 copy-start.7
  4.0 0.7 copy-start.8
  4.7 0.7 copy-start.9
  5.3 0.7 copy-start.10
  116.7 3.3 %copy-start.5 = (f32[2048]{0:T(1024)S(1)}, f32[2048]{0:T(1024)}, u32[]{:S(2)}) copy-start(f32[2048]{0:T(1024)} %param.12) | copy-start | bytes 24580
  116.7 3.3 %copy-start.6 = (f32[3,256]{1,0:T(4,128)S(1)}, f32[3,256]{1,0:T(4,128)}, u32[]{:S(2)}) copy-start(f32[3,256]{1,0:T(4,128)} %taps.1) | copy-start | bytes 9220
  120.0 2.2 %copy-start = (bf16[32,520,128]{2,1,0:T(8,128)(2,1)S(1)}, bf16[32,520,128]{2,1,0:T(8,128)(2,1)}, u32[]{:S(2)}) copy-start(bf16[32,520,128]{2,1,0:T(8,128)(2,1)} %convert_convert_fusion.pieces) | copy-start | bytes 12779524
  130.3 19.8 %collective-permute-start = (bf16[512,2048]{1,0:T(8,128)(2,1)S(1)}, bf16[512,2048]{1,0:T(8,128)(2,1)S(1)}, u32[]{:S(2)}, u32[]{:S(2)}) collective-permute-start(bf16[512,2048]{1,0:T(8,128)(2,1)S(1)} %multiply_convert_fusion), channel_id=1, source_target_pairs={{0,1},{1,0},{2,3},{3,2},{4,5},{5,4},{6,7},{7,6},{8,9},{9,8},{10,11... | collective-permute-start | bytes 6291464 | tf_op jit(solution)/shard_map/ppermute | solution.py:76

commit v3 on v2

--- a/solution.py
+++ b/solution.py
@@ -5,10 +5,12 @@
 from jax.experimental.pallas import tpu as pltpu
 from jax.sharding import PartitionSpec as P
 
+
 EPS = 1e-06
 LIFT = 2.0**18
 LOW = 2.0**12
 LANES = 128
+PARTS = 2
 ROWS = 256
 VMEM_BYTES = 28 * 2**20
 
@@ -42,7 +44,7 @@
         pack_kernel,
         out_shape=jax.ShapeDtypeStruct((total, LANES), jnp.float32),
         compiler_params=pltpu.CompilerParams(vmem_limit_bytes=4 * 2**20),
-    )(*weights, *scales)
+    )(*(pltpu.with_memory_space_constraint(a, pltpu.HBM) for a in (*weights, *scales)))
     pieces = lax.all_gather(packed.astype(jnp.float16), "fs")
     blocks = pieces.shape[1] // rows
     terms = [pieces[:, blocks * rows + k].astype(jnp.float32) for k in range(3)]
@@ -51,49 +53,66 @@
     for s in scales:
         columns.append(top[:, start : start + s.size].reshape(-1) * (1.0 / LIFT))
         start += s.size
-    pieces = lax.optimization_barrier(pieces.astype(jnp.float32).astype(jnp.bfloat16))
-    pieces = pltpu.with_memory_space_constraint(pieces, pltpu.VMEM)
-    return pieces, (jnp.concatenate(columns[:-1]), columns[-1])
+    each = blocks // PARTS * rows
+    parts = [
+        pieces[:, k * each : (k + 1) * each].astype(jnp.float32).astype(jnp.bfloat16)
+        for k in range(PARTS)
+    ]
+    return lax.optimization_barrier(parts), (jnp.concatenate(columns[:-1]), columns[-1])
 
 
 def summed_rows(left, weight, scale):
     count = lax.axis_size("tp")
     chips = count // 2
-    core = lax.axis_index("tp") % 2
+    me = lax.axis_index("tp")
+    chip, core = me // 2, me % 2
     rows = left.shape[0] // count
-    grid = left.reshape(chips, 2, rows, left.shape[1])
-
-    def part(which):
-        these = lax.dynamic_slice_in_dim(grid, which, 1, 1).reshape(chips * rows, -1)
-        return (
-            lax.dot_general(
-                these, weight, (((1,), (1,)), ((), ())), preferred_element_type=jnp.float32
-            )
-            * scale
-        ).astype(jnp.bfloat16)
+
+    def part(which, steps):
+        blocks = []
+        for step in steps:
+            target = 2 * lax.rem(chip + (1 - 2 * which) * step + chips, chips) + which
+            blocks.append(lax.dynamic_slice_in_dim(left, target * rows, rows, 0))
+        these = blocks[0] if len(blocks) == 1 else jnp.concatenate(blocks, axis=0)
+        total = lax.dot_general(
+            these, weight, (((1,), (1,)), ((), ())), preferred_element_type=jnp.float32
+        )
+        return (total * scale).astype(jnp.bfloat16)
+
+    def toward(sign):
+        return [(i, (i + sign * (2 - 4 * (i % 2))) % count) for i in range(count)]
+
+    def add(a, b):
+        return a.astype(jnp.float32) + b.astype(jnp.float32)
 
     swap = [(i, i ^ 1) for i in range(count)]
-    theirs = lax.ppermute(part(1 - core), "tp", swap)
-    pair = (part(core).astype(jnp.float32) + theirs.astype(jnp.float32)).astype(jnp.bfloat16)
-    same_core = [list(range(which, count, 2)) for which in range(2)]
-    parts = lax.all_to_all(
-        pair.reshape(chips, rows, -1), "tp", 0, 0, axis_index_groups=same_core
-    )
-    total = parts[0].astype(jnp.float32)
-    for k in range(1, chips):
-        total = total + parts[k].astype(jnp.float32)
-    return total.astype(jnp.bfloat16)
-
-
-def gate_kernel(tokens, gain, pieces, columns, taps, out, mixer, weight, carry):
+    theirs = lax.ppermute(part(1 - core, (2,)), "tp", swap)
+    far = add(part(core, (2,)), theirs).astype(jnp.bfloat16)
+    others = part(1 - core, (0, 1, 3))
+    far, others = lax.optimization_barrier((far, others))
+    carried = lax.ppermute(far, "tp", toward(1))
+    theirs = lax.ppermute(others, "tp", swap)
+    pair = add(part(core, (0, 1, 3)), theirs)
+    own, near, back = [pair[k * rows : (k + 1) * rows] for k in range(3)]
+    behind = lax.ppermute(back.astype(jnp.bfloat16), "tp", toward(-1))
+    onward = (near + carried.astype(jnp.float32)).astype(jnp.bfloat16)
+    ahead = lax.ppermute(onward, "tp", toward(1))
+    return (own + behind.astype(jnp.float32) + ahead.astype(jnp.float32)).astype(jnp.bfloat16)
+
+
+def gate_kernel(tokens, gain, columns, taps, *refs):
+    *pieces, out, mixer, weight, carry = refs
+
     @pl.when(pl.program_id(0) == 0)
     def _():
         carry[...] = jnp.zeros_like(carry)
         depth = weight.shape[0]
-        rows = depth // pieces.shape[0]
+        rows = depth // pieces[0].shape[0]
+        each = pieces[0].shape[1] // rows
         inputs = weight.shape[1] // LANES
         for k in range(inputs + mixer.shape[1] // LANES):
-            full = pieces[:, k * rows : (k + 1) * rows, :]
+            low = k % each * rows
+            full = pieces[k // each][:, low : low + rows, :]
             to, at = (weight, k) if k < inputs else (mixer, k - inputs)
             to[:, at * LANES : (at + 1) * LANES] = full.reshape(depth, LANES)
 
@@ -128,7 +147,7 @@
     return pl.pallas_call(
         gate_kernel,
         grid=(rows // ROWS,),
-        in_specs=[pl.BlockSpec((ROWS, depth), lambda i: (i, 0)), whole, whole, whole, whole],
+        in_specs=[pl.BlockSpec((ROWS, depth), lambda i: (i, 0))] + [whole] * (3 + len(pieces)),
         out_specs=[pl.BlockSpec((ROWS, width), lambda i: (i, 0)), whole],
         out_shape=[
             jax.ShapeDtypeStruct((rows, width), jnp.bfloat16),
@@ -141,7 +160,7 @@
         compiler_params=pltpu.CompilerParams(
             dimension_semantics=("arbitrary",), vmem_limit_bytes=VMEM_BYTES
         ),
-    )(pltpu.with_memory_space_constraint(tokens, pltpu.HBM), gain.reshape(1, -1), pieces, columns.reshape(1, -1), taps)
+    )(pltpu.with_memory_space_constraint(tokens, pltpu.HBM), gain.reshape(1, -1), columns.reshape(1, -1), taps, *pieces)
 
 
 def per_device(

time: 183 us -> 178 us (0.973)
  blocking collectives: 138 us -> 111 us
  waiting for transfers between devices: 3.76 us -> 18.2 us
  starting transfers between devices: 16 us -> 26.9 us
  local copies, waits for them, and re-layouts: 8.58 us -> 3.84 us
    all_to_all x1 -> x0, blocking collectives: 27.6 us -> none  [summed_rows(): lax.all_to_all(pair.reshape(chips, rows, -1), 'tp', 0, 0, axis_index_grou...]
    ppermute x1 -> x5, waiting for transfers between devices: 3.76 us -> 18.2 us  [the longest x1 7.18 us: summed_rows(): carried = lax.ppermute(far, 'tp', toward(1))]
    ppermute x1 -> x5, starting transfers between devices: 16 us -> 26.9 us  [the longest x1 16 us: summed_rows(): theirs = lax.ppermute(part(1 - core, (2,)), 'tp', swap)]
    unnamed x22 -> x8, local copies, waits for them, and re-layouts: 8.19 us -> 2.39 us
  transfers between devices with their start and end apart: 1 -> 5, of which waited for: 1 -> 4; matrix products, arithmetic and copies ran while one was open for 0% -> 1% of each run, Pallas kernels for 0% -> 0%
where the time goes in v3:
time: 178 us; the launch traced here: 175 us
  blocking collectives  111 us (62%)
  starting transfers between devices  26.9 us (15%)
  waiting for transfers between devices  18.2 us (10%)
  Pallas kernels  8.31 us (5%)
  local copies, waits for them, and re-layouts  3.84 us (2%)
  other arithmetic  3.82 us (2%)
  matrix products  3.03 us (2%)
    all_gather x1, blocking collectives, gathered(): pieces = lax.all_gather(packed.astype(jnp.float16), 'fs')  111 us
    ppermute x1, starting transfers between devices, summed_rows(): theirs = lax.ppermute(part(1 - core, (2,)), 'tp', swap)  16 us
    pallas_call x1, Pallas kernels, gated_rows(): pl.pallas_call(gate_kernel, grid=(rows // ROWS,), in_specs=[pl.BlockSpec(...  7.25 us
    ppermute x1, waiting for transfers between devices, summed_rows(): carried = lax.ppermute(far, 'tp', toward(1))  7.18 us
    ppermute x1, waiting for transfers between devices, summed_rows(): ahead = lax.ppermute(onward, 'tp', toward(1))  6.49 us
    ppermute x1, starting transfers between devices, summed_rows(): behind = lax.ppermute(back.astype(jnp.bfloat16), 'tp', toward(-1))  4.6 us
    ppermute x1, waiting for transfers between devices, summed_rows(): behind = lax.ppermute(back.astype(jnp.bfloat16), 'tp', toward(-1))  3.61 us
  transfers between devices with their start and end apart: 5, of which 4 were waited for; matrix products, arithmetic and copies ran while one was open for 1% of the time, Pallas kernels for 0%

profile of v3, /device:TPU:39, one launch (start us, length us, event | category | flops | bytes accessed | tf_op | source)
XLA Modules:
  0.0 175.1 jit_solution(1985027689783726707)
XLA Ops:
  0.0 1.1 shard_map.109
  1.1 110.6 %all-gather.2 = f16[16640,128]{1,0:T(8,128)(2,1)S(1)} all-gather(f16[520,128]{1,0:T(8,128)(2,1)S(1)} %convert_element_type.70), channel_id=2, replica_groups=mesh['grp'=2,'fs'=32,'tp'=8] {'fs'}, dimensions={0}, use_global_device_ids=true | all-gather | bytes 4392960 | tf_op jit(solution)/shard_map/all_gather | solution.py:48
  111.7 0.0 copy-start.2
  111.8 0.0 copy-start.3
  111.8 2.5 %convert_convert_fusion = (bf16[32,256,128]{2,1,0:T(8,128)(2,1)S(1)}, bf16[32,256,128]{2,1,0:T(8,128)(2,1)}) fusion(f16[32,520,128]{2,1,0:T(8,128)(2,1)S(1)} %bitcast.10), kind=kLoop, calls=%fused_computation | loop fusion | flops 4194304 | bytes 8388608 | tf_op jit(solution)/shard_map/convert_element_type | solution.py:58
  114.3 0.1 slice_multiply_fusion.3
  114.3 0.1 slice_multiply_fusion
  114.4 0.1 mul.141
  114.5 0.1 mul.139
  114.6 0.1 mul.137
  114.7 0.1 mul.152
  114.8 0.0 copy-done.2
  114.8 0.0 copy-done.3
  114.8 0.0 copy-start
  114.8 1.6 copy-done
  116.4 7.3 %shard_map.110 = (bf16[1024,256]{1,0:T(8,128)(2,1)S(1)}, bf16[2048,256]{1,0:T(8,128)(2,1)S(1)}) custom-call(bf16[1024,2048]{1,0:T(8,128)(2,1)} %tokens.1, f32[1,2048]{1,0:T(1,128)S(1)} %bitcast.8, f32[1,768]{1,0:T(1,128)S(1)} %reshape.31.columns, f32[3,256]{1,0:T(4,128)S(1)} %copy-done.3, bf16[32,256,128]{2,1,0:T(8,128)(2,1)S(1)} %copy-done, ...), custom_call_target="tpu_custom_call" | custom-call | tf_op jit(solution)/shard_map/pallas_call | solution.py:147
  123.6 0.0 copy-start.1
  123.7 0.8 copy-done.1
  124.4 0.5 fusion.2
  124.9 16.0 %collective-permute-start = (bf16[128,2048]{1,0:T(8,128)(2,1)S(1)}, bf16[128,2048]{1,0:T(8,128)(2,1)S(1)}, u32[]{:S(2)}, u32[]{:S(2)}) collective-permute-start(bf16[128,2048]{1,0:T(8,128)(2,1)S(1)} %fusion.2), channel_id=1, source_target_pairs={{0,1},{1,0},{2,3},{3,2},{4,5},{5,4},{6,7},{7,6},{8,9},{9,8},{10,11... | collective-permute-start | bytes 1572872 | tf_op jit(solution)/shard_map/ppermute | solution.py:89
  141.1 1.0 constant_dynamic-slice_fusion.5
  142.1 0.6 multiply_convert_fusion
  142.7 0.0 collective-permute-done
  142.7 1.3 add_convert_fusion
  144.1 2.0 %collective-permute-start.1 = (bf16[384,2048]{1,0:T(8,128)(2,1)S(1)}, bf16[384,2048]{1,0:T(8,128)(2,1)S(1)}, u32[]{:S(2)}, u32[]{:S(2)}) collective-permute-start(bf16[384,2048]{1,0:T(8,128)(2,1)S(1)} %multiply_convert_fusion), channel_id=1, source_target_pairs={{0,1},{1,0},{2,3},{3,2},{4,5},{5,4},{6,7},{7,6},{8,9},{9,8},{10,11... | collective-permute-start | bytes 4718600 | tf_op jit(solution)/shard_map/ppermute | solution.py:94
  146.1 2.3 %collective-permute-start.3 = (bf16[128,2048]{1,0:T(8,128)(2,1)S(1)}, bf16[128,2048]{1,0:T(8,128)(2,1)S(1)}, u32[]{:S(2)}, u32[]{:S(2)}) collective-permute-start(bf16[128,2048]{1,0:T(8,128)(2,1)S(1)} %add_convert_fusion), channel_id=1, source_target_pairs={{0,2},{1,7},{2,4},{3,1},{4,6},{5,3},{6,0},{7,5},{8,10},{9,15},{10,... | collective-permute-start | bytes 1572872 | tf_op jit(solution)/shard_map/ppermute | solution.py:93
  148.4 0.9 collective-permute-done.1
  149.4 0.6 convert_add_fusion
  150.0 0.1 slice.89
  150.1 7.2 %collective-permute-done.3 = bf16[128,2048]{1,0:T(8,128)(2,1)S(1)} collective-permute-done((bf16[128,2048]{1,0:T(8,128)(2,1)S(1)}, bf16[128,2048]{1,0:T(8,128)(2,1)S(1)}, u32[]{:S(2)}, u32[]{:S(2)}) %collective-permute-start.3) | collective-permute-done | bytes 524320 | tf_op jit(solution)/shard_map/ppermute | solution.py:93
  157.3 0.1 fusion.3
  157.4 2.0 %collective-permute-start.4 = (bf16[128,2048]{1,0:T(8,128)(2,1)S(1)}, bf16[128,2048]{1,0:T(8,128)(2,1)S(1)}, u32[]{:S(2)}, u32[]{:S(2)}) collective-permute-start(bf16[128,2048]{1,0:T(8,128)(2,1)S(1)} %fusion.3), channel_id=1, source_target_pairs={{0,2},{1,7},{2,4},{3,1},{4,6},{5,3},{6,0},{7,5},{8,10},{9,15},{10,... | collective-permute-start | bytes 1572872 | tf_op jit(solution)/shard_map/ppermute | solution.py:99
  159.3 4.6 %collective-permute-start.2 = (bf16[128,2048]{1,0:T(8,128)(2,1)S(1)}, bf16[128,2048]{1,0:T(8,128)(2,1)S(1)}, u32[]{:S(2)}, u32[]{:S(2)}) collective-permute-start(bf16[128,2048]{1,0:T(8,128)(2,1)S(1)} %slice.89), channel_id=1, source_target_pairs={{0,6},{1,3},{2,0},{3,5},{4,2},{5,7},{6,4},{7,1},{8,14},{9,11},{10,... | collective-permute-start | bytes 1572872 | tf_op jit(solution)/shard_map/ppermute | solution.py:97
  164.0 6.5 %collective-permute-done.4 = bf16[128,2048]{1,0:T(8,128)(2,1)S(1)} collective-permute-done((bf16[128,2048]{1,0:T(8,128)(2,1)S(1)}, bf16[128,2048]{1,0:T(8,128)(2,1)S(1)}, u32[]{:S(2)}, u32[]{:S(2)}) %collective-permute-start.4) | collective-permute-done | bytes 524320 | tf_op jit(solution)/shard_map/ppermute | solution.py:99
  170.4 3.6 %collective-permute-done.2 = bf16[128,2048]{1,0:T(8,128)(2,1)S(1)} collective-permute-done((bf16[128,2048]{1,0:T(8,128)(2,1)S(1)}, bf16[128,2048]{1,0:T(8,128)(2,1)S(1)}, u32[]{:S(2)}, u32[]{:S(2)}) %collective-permute-start.2) | collective-permute-done | bytes 524320 | tf_op jit(solution)/shard_map/ppermute | solution.py:97
  174.1 1.0 fusion.5
  (4 shorter events, 0.1 us)
Async XLA Ops:
  111.7 3.0 %copy-start.2 = (f32[2048]{0:T(1024)S(1)}, f32[2048]{0:T(1024)}, u32[]{:S(2)}) copy-start(f32[2048]{0:T(1024)} %param.12) | copy-start | bytes 24580
  111.8 3.0 %copy-start.3 = (f32[3,256]{1,0:T(4,128)S(1)}, f32[3,256]{1,0:T(4,128)}, u32[]{:S(2)}) copy-start(f32[3,256]{1,0:T(4,128)} %taps.1) | copy-start | bytes 9220
  114.8 1.6 copy-start
  123.6 0.8 copy-start.1
  124.9 17.8 %collective-permute-start = (bf16[128,2048]{1,0:T(8,128)(2,1)S(1)}, bf16[128,2048]{1,0:T(8,128)(2,1)S(1)}, u32[]{:S(2)}, u32[]{:S(2)}) collective-permute-start(bf16[128,2048]{1,0:T(8,128)(2,1)S(1)} %fusion.2), channel_id=1, source_target_pairs={{0,1},{1,0},{2,3},{3,2},{4,5},{5,4},{6,7},{7,6},{8,9},{9,8},{10,11... | collective-permute-start | bytes 1572872 | tf_op jit(solution)/shard_map/ppermute | solution.py:89
  144.1 5.3 %collective-permute-start.1 = (bf16[384,2048]{1,0:T(8,128)(2,1)S(1)}, bf16[384,2048]{1,0:T(8,128)(2,1)S(1)}, u32[]{:S(2)}, u32[]{:S(2)}) collective-permute-start(bf16[384,2048]{1,0:T(8,128)(2,1)S(1)} %multiply_convert_fusion), channel_id=1, source_target_pairs={{0,1},{1,0},{2,3},{3,2},{4,5},{5,4},{6,7},{7,6},{8,9},{9,8},{10,11... | collective-permute-start | bytes 4718600 | tf_op jit(solution)/shard_map/ppermute | solution.py:94
  146.1 11.2 %collective-permute-start.3 = (bf16[128,2048]{1,0:T(8,128)(2,1)S(1)}, bf16[128,2048]{1,0:T(8,128)(2,1)S(1)}, u32[]{:S(2)}, u32[]{:S(2)}) collective-permute-start(bf16[128,2048]{1,0:T(8,128)(2,1)S(1)} %add_convert_fusion), channel_id=1, source_target_pairs={{0,2},{1,7},{2,4},{3,1},{4,6},{5,3},{6,0},{7,5},{8,10},{9,15},{10,... | collective-permute-start | bytes 1572872 | tf_op jit(solution)/shard_map/ppermute | solution.py:93
  157.4 13.1 %collective-permute-start.4 = (bf16[128,2048]{1,0:T(8,128)(2,1)S(1)}, bf16[128,2048]{1,0:T(8,128)(2,1)S(1)}, u32[]{:S(2)}, u32[]{:S(2)}) collective-permute-start(bf16[128,2048]{1,0:T(8,128)(2,1)S(1)} %fusion.3), channel_id=1, source_target_pairs={{0,2},{1,7},{2,4},{3,1},{4,6},{5,3},{6,0},{7,5},{8,10},{9,15},{10,... | collective-permute-start | bytes 1572872 | tf_op jit(solution)/shard_map/ppermute | solution.py:99
  159.3 14.7 %collective-permute-start.2 = (bf16[128,2048]{1,0:T(8,128)(2,1)S(1)}, bf16[128,2048]{1,0:T(8,128)(2,1)S(1)}, u32[]{:S(2)}, u32[]{:S(2)}) collective-permute-start(bf16[128,2048]{1,0:T(8,128)(2,1)S(1)} %slice.89), channel_id=1, source_target_pairs={{0,6},{1,3},{2,0},{3,5},{4,2},{5,7},{6,4},{7,1},{8,14},{9,11},{10,... | collective-permute-start | bytes 1572872 | tf_op jit(solution)/shard_map/ppermute | solution.py:97

commit v4 on v3

--- a/solution.py
+++ b/solution.py
@@ -86,18 +86,18 @@
         return a.astype(jnp.float32) + b.astype(jnp.float32)
 
     swap = [(i, i ^ 1) for i in range(count)]
-    theirs = lax.ppermute(part(1 - core, (2,)), "tp", swap)
-    far = add(part(core, (2,)), theirs).astype(jnp.bfloat16)
-    others = part(1 - core, (0, 1, 3))
-    far, others = lax.optimization_barrier((far, others))
-    carried = lax.ppermute(far, "tp", toward(1))
+    theirs = lax.ppermute(part(1 - core, (2, 3)), "tp", swap)
+    outward = add(part(core, (2, 3)), theirs).astype(jnp.bfloat16)
+    others = part(1 - core, (0, 1))
+    outward, others = lax.optimization_barrier((outward, others))
+    carried = lax.ppermute(outward[:rows], "tp", toward(1))
+    behind = lax.ppermute(outward[rows:], "tp", toward(-1))
     theirs = lax.ppermute(others, "tp", swap)
-    pair = add(part(core, (0, 1, 3)), theirs)
-    own, near, back = [pair[k * rows : (k + 1) * rows] for k in range(3)]
-    behind = lax.ppermute(back.astype(jnp.bfloat16), "tp", toward(-1))
-    onward = (near + carried.astype(jnp.float32)).astype(jnp.bfloat16)
+    pair = add(part(core, (0, 1)), theirs)
+    own = pair[:rows].astype(jnp.bfloat16)
+    onward = (pair[rows:] + carried.astype(jnp.float32)).astype(jnp.bfloat16)
     ahead = lax.ppermute(onward, "tp", toward(1))
-    return (own + behind.astype(jnp.float32) + ahead.astype(jnp.float32)).astype(jnp.bfloat16)
+    return (add(own, behind) + ahead.astype(jnp.float32)).astype(jnp.bfloat16)
 
 
 def gate_kernel(tokens, gain, columns, taps, *refs):

time: 178 us -> 174 us (0.978)
    ppermute x1, waiting for transfers between devices: 6.49 us -> 9.2 us  [summed_rows(): ahead = lax.ppermute(onward, 'tp', toward(1))]
  transfers between devices with their start and end apart: 5 -> 5, of which waited for: 4 -> 3; matrix products, arithmetic and copies ran while one was open for 1% -> 1% of each run, Pallas kernels for 0% -> 0%
where the time goes in v4:
time: 174 us; the launch traced here: 173 us
  blocking collectives  111 us (64%)
  starting transfers between devices  26.8 us (15%)
  waiting for transfers between devices  18.5 us (11%)
  Pallas kernels  8.32 us (5%)
  other arithmetic  4.16 us (2%)
  local copies, waits for them, and re-layouts  2.09 us (1%)
  matrix products  1.89 us (1%)
    all_gather x1, blocking collectives, gathered(): pieces = lax.all_gather(packed.astype(jnp.float16), 'fs')  111 us
    ppermute x1, starting transfers between devices, summed_rows(): theirs = lax.ppermute(part(1 - core, (2, 3)), 'tp', swap)  16 us
    ppermute x1, waiting for transfers between devices, summed_rows(): ahead = lax.ppermute(onward, 'tp', toward(1))  9.2 us
    ppermute x1, waiting for transfers between devices, summed_rows(): carried = lax.ppermute(outward[:rows], 'tp', toward(1))  7.5 us
    pallas_call x1, Pallas kernels, gated_rows(): pl.pallas_call(gate_kernel, grid=(rows // ROWS,), in_specs=[pl.BlockSpec(...  7.27 us
    ppermute x1, starting transfers between devices, summed_rows(): behind = lax.ppermute(outward[rows:], 'tp', toward(-1))  4.19 us
  transfers between devices with their start and end apart: 5, of which 3 were waited for; matrix products, arithmetic and copies ran while one was open for 1% of the time, Pallas kernels for 0%

profile of v4, /device:TPU:39, one launch (start us, length us, event | category | flops | bytes accessed | tf_op | source)
XLA Modules:
  0.0 172.6 jit_solution(3983027565367820136)
XLA Ops:
  0.0 1.1 shard_map.109
  1.1 110.6 %all-gather.2 = f16[16640,128]{1,0:T(8,128)(2,1)S(1)} all-gather(f16[520,128]{1,0:T(8,128)(2,1)S(1)} %convert_element_type.73), channel_id=2, replica_groups=mesh['grp'=2,'fs'=32,'tp'=8] {'fs'}, dimensions={0}, use_global_device_ids=true | all-gather | bytes 4392960 | tf_op jit(solution)/shard_map/all_gather | solution.py:48
  111.7 0.0 copy-start.1
  111.8 0.0 copy-start.2
  111.8 2.5 %convert_convert_fusion = (bf16[32,256,128]{2,1,0:T(8,128)(2,1)S(1)}, bf16[32,256,128]{2,1,0:T(8,128)(2,1)}) fusion(f16[32,520,128]{2,1,0:T(8,128)(2,1)S(1)} %bitcast.10), kind=kLoop, calls=%fused_computation | loop fusion | flops 4194304 | bytes 8388608 | tf_op jit(solution)/shard_map/convert_element_type | solution.py:58
  114.3 0.1 slice_multiply_fusion.3
  114.3 0.1 slice_multiply_fusion
  114.5 0.1 mul.139
  114.6 0.1 mul.137
  114.6 0.1 mul.135
  114.8 0.1 mul.147
  114.8 0.0 copy-done.1
  114.8 0.0 copy-done.2
  114.8 0.0 copy-start
  114.9 1.6 copy-done
  116.4 7.3 %shard_map.110 = (bf16[1024,256]{1,0:T(8,128)(2,1)S(1)}, bf16[2048,256]{1,0:T(8,128)(2,1)S(1)}) custom-call(bf16[1024,2048]{1,0:T(8,128)(2,1)} %tokens.1, f32[1,2048]{1,0:T(1,128)S(1)} %bitcast.8, f32[1,768]{1,0:T(1,128)S(1)} %reshape.31.columns, f32[3,256]{1,0:T(4,128)S(1)} %copy-done.2, bf16[32,256,128]{2,1,0:T(8,128)(2,1)S(1)} %copy-done, ...), custom_call_target="tpu_custom_call" | custom-call | tf_op jit(solution)/shard_map/pallas_call | solution.py:147
  123.7 0.1 constant_dynamic-slice_fusion.1
  123.8 0.5 fusion.4
  124.3 16.0 %collective-permute-start = (bf16[256,2048]{1,0:T(8,128)(2,1)S(1)}, bf16[256,2048]{1,0:T(8,128)(2,1)S(1)}, u32[]{:S(2)}, u32[]{:S(2)}) collective-permute-start(bf16[256,2048]{1,0:T(8,128)(2,1)S(1)} %fusion.4), channel_id=1, source_target_pairs={{0,1},{1,0},{2,3},{3,2},{4,5},{5,4},{6,7},{7,6},{8,9},{9,8},{10,11... | collective-permute-start | bytes 3145736 | tf_op jit(solution)/shard_map/ppermute | solution.py:89
  140.2 0.5 fusion.5
  140.7 1.8 %collective-permute-done = bf16[256,2048]{1,0:T(8,128)(2,1)S(1)} collective-permute-done((bf16[256,2048]{1,0:T(8,128)(2,1)S(1)}, bf16[256,2048]{1,0:T(8,128)(2,1)S(1)}, u32[]{:S(2)}, u32[]{:S(2)}) %collective-permute-start) | collective-permute-done | bytes 1048608 | tf_op jit(solution)/shard_map/ppermute | solution.py:89
  142.5 0.5 add_convert_fusion
  143.0 2.3 %collective-permute-start.1 = (bf16[256,2048]{1,0:T(8,128)(2,1)S(1)}, bf16[256,2048]{1,0:T(8,128)(2,1)S(1)}, u32[]{:S(2)}, u32[]{:S(2)}) collective-permute-start(bf16[256,2048]{1,0:T(8,128)(2,1)S(1)} %fusion.5), channel_id=1, source_target_pairs={{0,1},{1,0},{2,3},{3,2},{4,5},{5,4},{6,7},{7,6},{8,9},{9,8},{10,11... | collective-permute-start | bytes 3145736 | tf_op jit(solution)/shard_map/ppermute | solution.py:95
  145.3 0.5 fusion.1
  145.8 0.1 fusion.26
  145.9 2.4 %collective-permute-start.3 = (bf16[128,2048]{1,0:T(8,128)(2,1)S(1)}, bf16[128,2048]{1,0:T(8,128)(2,1)S(1)}, u32[]{:S(2)}, u32[]{:S(2)}) collective-permute-start(bf16[128,2048]{1,0:T(8,128)(2,1)S(1)} %get-tuple-element.20), channel_id=1, source_target_pairs={{0,2},{1,7},{2,4},{3,1},{4,6},{5,3},{6,0},{7,5},{8,10},{9,15},{10,... | collective-permute-start | bytes 1572872 | tf_op jit(solution)/shard_map/ppermute | solution.py:93
  148.3 4.2 %collective-permute-start.2 = (bf16[128,2048]{1,0:T(8,128)(2,1)S(1)}, bf16[128,2048]{1,0:T(8,128)(2,1)S(1)}, u32[]{:S(2)}, u32[]{:S(2)}) collective-permute-start(bf16[128,2048]{1,0:T(8,128)(2,1)S(1)} %get-tuple-element.19), channel_id=1, source_target_pairs={{0,6},{1,3},{2,0},{3,5},{4,2},{5,7},{6,4},{7,1},{8,14},{9,11},{10,... | collective-permute-start | bytes 1572872 | tf_op jit(solution)/shard_map/ppermute | solution.py:94
  152.5 0.0 collective-permute-done.1
  152.5 0.4 convert_add_fusion
  152.9 7.5 %collective-permute-done.3 = bf16[128,2048]{1,0:T(8,128)(2,1)S(1)} collective-permute-done((bf16[128,2048]{1,0:T(8,128)(2,1)S(1)}, bf16[128,2048]{1,0:T(8,128)(2,1)S(1)}, u32[]{:S(2)}, u32[]{:S(2)}) %collective-permute-start.3) | collective-permute-done | bytes 524320 | tf_op jit(solution)/shard_map/ppermute | solution.py:93
  160.4 0.1 fusion.6
  160.5 2.0 %collective-permute-start.4 = (bf16[128,2048]{1,0:T(8,128)(2,1)S(1)}, bf16[128,2048]{1,0:T(8,128)(2,1)S(1)}, u32[]{:S(2)}, u32[]{:S(2)}) collective-permute-start(bf16[128,2048]{1,0:T(8,128)(2,1)S(1)} %fusion.6), channel_id=1, source_target_pairs={{0,2},{1,7},{2,4},{3,1},{4,6},{5,3},{6,0},{7,5},{8,10},{9,15},{10,... | collective-permute-start | bytes 1572872 | tf_op jit(solution)/shard_map/ppermute | solution.py:99
  162.4 0.0 collective-permute-done.2
  162.4 9.2 %collective-permute-done.4 = bf16[128,2048]{1,0:T(8,128)(2,1)S(1)} collective-permute-done((bf16[128,2048]{1,0:T(8,128)(2,1)S(1)}, bf16[128,2048]{1,0:T(8,128)(2,1)S(1)}, u32[]{:S(2)}, u32[]{:S(2)}) %collective-permute-start.4) | collective-permute-done | bytes 524320 | tf_op jit(solution)/shard_map/ppermute | solution.py:99
  171.6 1.0 add_convert_fusion.1
  (4 shorter events, 0.1 us)
Async XLA Ops:
  111.7 3.1 %copy-start.1 = (f32[2048]{0:T(1024)S(1)}, f32[2048]{0:T(1024)}, u32[]{:S(2)}) copy-start(f32[2048]{0:T(1024)} %param.12) | copy-start | bytes 24580
  111.8 3.1 %copy-start.2 = (f32[3,256]{1,0:T(4,128)S(1)}, f32[3,256]{1,0:T(4,128)}, u32[]{:S(2)}) copy-start(f32[3,256]{1,0:T(4,128)} %taps.1) | copy-start | bytes 9220
  114.8 1.6 copy-start
  124.3 18.3 %collective-permute-start = (bf16[256,2048]{1,0:T(8,128)(2,1)S(1)}, bf16[256,2048]{1,0:T(8,128)(2,1)S(1)}, u32[]{:S(2)}, u32[]{:S(2)}) collective-permute-start(bf16[256,2048]{1,0:T(8,128)(2,1)S(1)} %fusion.4), channel_id=1, source_target_pairs={{0,1},{1,0},{2,3},{3,2},{4,5},{5,4},{6,7},{7,6},{8,9},{9,8},{10,11... | collective-permute-start | bytes 3145736 | tf_op jit(solution)/shard_map/ppermute | solution.py:89
  143.0 9.5 %collective-permute-start.1 = (bf16[256,2048]{1,0:T(8,128)(2,1)S(1)}, bf16[256,2048]{1,0:T(8,128)(2,1)S(1)}, u32[]{:S(2)}, u32[]{:S(2)}) collective-permute-start(bf16[256,2048]{1,0:T(8,128)(2,1)S(1)} %fusion.5), channel_id=1, source_target_pairs={{0,1},{1,0},{2,3},{3,2},{4,5},{5,4},{6,7},{7,6},{8,9},{9,8},{10,11... | collective-permute-start | bytes 3145736 | tf_op jit(solution)/shard_map/ppermute | solution.py:95
  145.9 14.4 %collective-permute-start.3 = (bf16[128,2048]{1,0:T(8,128)(2,1)S(1)}, bf16[128,2048]{1,0:T(8,128)(2,1)S(1)}, u32[]{:S(2)}, u32[]{:S(2)}) collective-permute-start(bf16[128,2048]{1,0:T(8,128)(2,1)S(1)} %get-tuple-element.20), channel_id=1, source_target_pairs={{0,2},{1,7},{2,4},{3,1},{4,6},{5,3},{6,0},{7,5},{8,10},{9,15},{10,... | collective-permute-start | bytes 1572872 | tf_op jit(solution)/shard_map/ppermute | solution.py:93
  148.3 14.1 %collective-permute-start.2 = (bf16[128,2048]{1,0:T(8,128)(2,1)S(1)}, bf16[128,2048]{1,0:T(8,128)(2,1)S(1)}, u32[]{:S(2)}, u32[]{:S(2)}) collective-permute-start(bf16[128,2048]{1,0:T(8,128)(2,1)S(1)} %get-tuple-element.19), channel_id=1, source_target_pairs={{0,6},{1,3},{2,0},{3,5},{4,2},{5,7},{6,4},{7,1},{8,14},{9,11},{10,... | collective-permute-start | bytes 1572872 | tf_op jit(solution)/shard_map/ppermute | solution.py:94
  160.5 11.2 %collective-permute-start.4 = (bf16[128,2048]{1,0:T(8,128)(2,1)S(1)}, bf16[128,2048]{1,0:T(8,128)(2,1)S(1)}, u32[]{:S(2)}, u32[]{:S(2)}) collective-permute-start(bf16[128,2048]{1,0:T(8,128)(2,1)S(1)} %fusion.6), channel_id=1, source_target_pairs={{0,2},{1,7},{2,4},{3,1},{4,6},{5,3},{6,0},{7,5},{8,10},{9,15},{10,... | collective-permute-start | bytes 1572872 | tf_op jit(solution)/shard_map/ppermute | solution.py:99

commit v5 on v4

--- a/solution.py
+++ b/solution.py
@@ -11,8 +11,9 @@
 LOW = 2.0**12
 LANES = 128
 PARTS = 2
-ROWS = 256
-VMEM_BYTES = 28 * 2**20
+ROWS = 512
+SUB = 128
+VMEM_BYTES = 32 * 2**20
 
 
 def pack_kernel(*refs):
@@ -101,53 +102,63 @@
 
 
 def gate_kernel(tokens, gain, columns, taps, *refs):
-    *pieces, out, mixer, weight, carry = refs
+    *pieces, far_piece, out, mixer, weight, carry, near_piece, ready = refs
+    width = out.shape[1]
 
     @pl.when(pl.program_id(0) == 0)
     def _():
+        fetch = pltpu.make_async_copy(far_piece, near_piece, ready)
+        fetch.start()
         carry[...] = jnp.zeros_like(carry)
         depth = weight.shape[0]
-        rows = depth // pieces[0].shape[0]
-        each = pieces[0].shape[1] // rows
-        inputs = weight.shape[1] // LANES
-        for k in range(inputs + mixer.shape[1] // LANES):
-            low = k % each * rows
-            full = pieces[k // each][:, low : low + rows, :]
-            to, at = (weight, k) if k < inputs else (mixer, k - inputs)
-            to[:, at * LANES : (at + 1) * LANES] = full.reshape(depth, LANES)
-
-    values = tokens[...].astype(jnp.float32)
-    inverse = lax.rsqrt(jnp.mean(values * values, axis=-1, keepdims=True) + EPS)
-    normal = (values * inverse * gain[...]).astype(jnp.bfloat16)
-    width = out.shape[1]
-
-    def projected(at):
-        cols = slice(at * width, (at + 1) * width)
-        total = jnp.dot(normal, weight[:, cols], preferred_element_type=jnp.float32)
-        return (total * columns[:, cols]).astype(jnp.bfloat16).astype(jnp.float32)
-
-    product = projected(1) * projected(2)
+        rows = depth // near_piece.shape[0]
+        inputs, at = weight.shape[1] // LANES, 0
+        for piece in (*pieces, near_piece):
+            if piece is near_piece:
+                fetch.wait()
+            for low in range(0, piece.shape[1], rows):
+                full = piece[:, low : low + rows, :].reshape(depth, LANES)
+                to, k = (weight, at) if at < inputs else (mixer, at - inputs)
+                to[:, k * LANES : (k + 1) * LANES] = full
+                at += 1
+
     last = carry[...]
-    carry[...] = product[-8:]
     row = lax.broadcasted_iota(jnp.int32, (8, width), 0)
-
-    def shifted(by):
-        moved = pltpu.roll(product, by, 0)
-        head = jnp.where(row < by, pltpu.roll(last, by, 0), moved[:8])
-        return jnp.concatenate([head, moved[8:]], axis=0)
-
-    filtered = taps[0:1] * shifted(2) + taps[1:2] * shifted(1) + taps[2:3] * product
-    out[...] = (projected(0) * filtered).astype(jnp.bfloat16)
+    for low in range(0, ROWS, SUB):
+        values = tokens[low : low + SUB, :].astype(jnp.float32)
+        inverse = lax.rsqrt(jnp.mean(values * values, axis=-1, keepdims=True) + EPS)
+        normal = (values * inverse * gain[...]).astype(jnp.bfloat16)
+
+        def projected(at):
+            cols = slice(at * width, (at + 1) * width)
+            total = jnp.dot(normal, weight[:, cols], preferred_element_type=jnp.float32)
+            return (total * columns[:, cols]).astype(jnp.bfloat16).astype(jnp.float32)
+
+        product = projected(1) * projected(2)
+
+        def shifted(by):
+            moved = pltpu.roll(product, by, 0)
+            head = jnp.where(row < by, pltpu.roll(last, by, 0), moved[:8])
+            return jnp.concatenate([head, moved[8:]], axis=0)
+
+        filtered = taps[0:1] * shifted(2) + taps[1:2] * shifted(1) + taps[2:3] * product
+        out[low : low + SUB, :] = (projected(0) * filtered).astype(jnp.bfloat16)
+        last = product[-8:]
+    carry[...] = last
 
 
 def gated_rows(tokens, gain, pieces, columns, taps):
     rows, depth = tokens.shape
     width = taps.shape[1]
     whole = pl.BlockSpec(memory_space=pltpu.VMEM)
+    hbm = pl.BlockSpec(memory_space=pltpu.HBM)
+    *pieces, far_piece = pieces
     return pl.pallas_call(
         gate_kernel,
         grid=(rows // ROWS,),
-        in_specs=[pl.BlockSpec((ROWS, depth), lambda i: (i, 0))] + [whole] * (3 + len(pieces)),
+        in_specs=[pl.BlockSpec((ROWS, depth), lambda i: (i, 0))]
+        + [whole] * (3 + len(pieces))
+        + [hbm],
         out_specs=[pl.BlockSpec((ROWS, width), lambda i: (i, 0)), whole],
         out_shape=[
             jax.ShapeDtypeStruct((rows, width), jnp.bfloat16),
@@ -156,11 +167,20 @@
         scratch_shapes=[
             pltpu.VMEM((depth, 3 * width), jnp.bfloat16),
             pltpu.VMEM((8, width), jnp.float32),
+            pltpu.VMEM(far_piece.shape, far_piece.dtype),
+            pltpu.SemaphoreType.DMA,
         ],
         compiler_params=pltpu.CompilerParams(
             dimension_semantics=("arbitrary",), vmem_limit_bytes=VMEM_BYTES
         ),
-    )(pltpu.with_memory_space_constraint(tokens, pltpu.HBM), gain.reshape(1, -1), columns.reshape(1, -1), taps, *pieces)
+    )(
+        pltpu.with_memory_space_constraint(tokens, pltpu.HBM),
+        gain.reshape(1, -1),
+        columns.reshape(1, -1),
+        taps,
+        *pieces,
+        pltpu.with_memory_space_constraint(far_piece, pltpu.HBM),
+    )
 
 
 def per_device(

time: 174 us -> 173 us (level)
  no operation moved by 1% of the time
where the time goes in v5:
time: 173 us; the launch traced here: 172 us
  blocking collectives  111 us (64%)
  starting transfers between devices  26.8 us (15%)
  waiting for transfers between devices  18.5 us (11%)
  Pallas kernels  9.02 us (5%)
  other arithmetic  4.16 us (2%)
  matrix products  1.89 us (1%)
    all_gather x1, blocking collectives, gathered(): pieces = lax.all_gather(packed.astype(jnp.float16), 'fs')  111 us
    ppermute x1, starting transfers between devices, summed_rows(): theirs = lax.ppermute(part(1 - core, (2, 3)), 'tp', swap)  16 us
    ppermute x1, waiting for transfers between devices, summed_rows(): ahead = lax.ppermute(onward, 'tp', toward(1))  9.2 us
    pallas_call x1, Pallas kernels, gated_rows(): pl.pallas_call(gate_kernel, grid=(rows // ROWS,), in_specs=[pl.BlockSpec(...  7.97 us
    ppermute x1, waiting for transfers between devices, summed_rows(): carried = lax.ppermute(outward[:rows], 'tp', toward(1))  7.52 us
    ppermute x1, starting transfers between devices, summed_rows(): behind = lax.ppermute(outward[rows:], 'tp', toward(-1))  4.2 us
  transfers between devices with their start and end apart: 5, of which 3 were waited for; matrix products, arithmetic and copies ran while one was open for 1% of the time, Pallas kernels for 0%

profile of v5, /device:TPU:39, one launch (start us, length us, event | category | flops | bytes accessed | tf_op | source)
XLA Modules:
  0.0 171.8 jit_solution(13939123759253016184)
XLA Ops:
  0.0 1.1 shard_map.109
  1.1 110.6 %all-gather.2 = f16[16640,128]{1,0:T(8,128)(2,1)S(1)} all-gather(f16[520,128]{1,0:T(8,128)(2,1)S(1)} %convert_element_type.73), channel_id=2, replica_groups=mesh['grp'=2,'fs'=32,'tp'=8] {'fs'}, dimensions={0}, use_global_device_ids=true | all-gather | bytes 4392960 | tf_op jit(solution)/shard_map/all_gather | solution.py:49
  111.7 0.0 copy-start
  111.8 0.0 copy-start.1
  111.8 2.5 %convert_convert_fusion = (bf16[32,256,128]{2,1,0:T(8,128)(2,1)}, bf16[32,256,128]{2,1,0:T(8,128)(2,1)S(1)}) fusion(f16[32,520,128]{2,1,0:T(8,128)(2,1)S(1)} %bitcast.10), kind=kLoop, calls=%fused_computation | loop fusion | flops 4194304 | bytes 8388608 | tf_op jit(solution)/shard_map/convert_element_type | solution.py:59
  114.3 0.1 slice_multiply_fusion.3
  114.3 0.1 slice_multiply_fusion
  114.5 0.1 mul.139
  114.6 0.1 mul.137
  114.7 0.1 mul.135
  114.8 0.1 mul.147
  114.8 0.0 copy-done
  114.8 0.0 copy-done.1
  114.8 8.0 %shard_map.110 = (bf16[1024,256]{1,0:T(8,128)(2,1)S(1)}, bf16[2048,256]{1,0:T(8,128)(2,1)S(1)}) custom-call(bf16[1024,2048]{1,0:T(8,128)(2,1)} %tokens.1, f32[1,2048]{1,0:T(1,128)S(1)} %bitcast.8, f32[1,768]{1,0:T(1,128)S(1)} %reshape.31.columns, f32[3,256]{1,0:T(4,128)S(1)} %copy-done.1, bf16[32,256,128]{2,1,0:T(8,128)(2,1)S(1)} %get-tuple-element.11.refs_0_, ...), custom_call_target="tpu_custom_call" | custom-call | tf_op jit(solution)/shard_map/pallas_call | solution.py:156
  122.8 0.1 constant_dynamic-slice_fusion.1
  122.9 0.5 fusion.4
  123.4 16.0 %collective-permute-start = (bf16[256,2048]{1,0:T(8,128)(2,1)S(1)}, bf16[256,2048]{1,0:T(8,128)(2,1)S(1)}, u32[]{:S(2)}, u32[]{:S(2)}) collective-permute-start(bf16[256,2048]{1,0:T(8,128)(2,1)S(1)} %fusion.4), channel_id=1, source_target_pairs={{0,1},{1,0},{2,3},{3,2},{4,5},{5,4},{6,7},{7,6},{8,9},{9,8},{10,11... | collective-permute-start | bytes 3145736 | tf_op jit(solution)/shard_map/ppermute | solution.py:90
  139.4 0.5 fusion.5
  139.9 1.8 %collective-permute-done = bf16[256,2048]{1,0:T(8,128)(2,1)S(1)} collective-permute-done((bf16[256,2048]{1,0:T(8,128)(2,1)S(1)}, bf16[256,2048]{1,0:T(8,128)(2,1)S(1)}, u32[]{:S(2)}, u32[]{:S(2)}) %collective-permute-start) | collective-permute-done | bytes 1048608 | tf_op jit(solution)/shard_map/ppermute | solution.py:90
  141.6 0.5 add_convert_fusion
  142.1 2.3 %collective-permute-start.1 = (bf16[256,2048]{1,0:T(8,128)(2,1)S(1)}, bf16[256,2048]{1,0:T(8,128)(2,1)S(1)}, u32[]{:S(2)}, u32[]{:S(2)}) collective-permute-start(bf16[256,2048]{1,0:T(8,128)(2,1)S(1)} %fusion.5), channel_id=1, source_target_pairs={{0,1},{1,0},{2,3},{3,2},{4,5},{5,4},{6,7},{7,6},{8,9},{9,8},{10,11... | collective-permute-start | bytes 3145736 | tf_op jit(solution)/shard_map/ppermute | solution.py:96
  144.5 0.5 fusion.1
  144.9 0.1 fusion.26
  145.0 2.4 %collective-permute-start.3 = (bf16[128,2048]{1,0:T(8,128)(2,1)S(1)}, bf16[128,2048]{1,0:T(8,128)(2,1)S(1)}, u32[]{:S(2)}, u32[]{:S(2)}) collective-permute-start(bf16[128,2048]{1,0:T(8,128)(2,1)S(1)} %get-tuple-element.20), channel_id=1, source_target_pairs={{0,2},{1,7},{2,4},{3,1},{4,6},{5,3},{6,0},{7,5},{8,10},{9,15},{10,... | collective-permute-start | bytes 1572872 | tf_op jit(solution)/shard_map/ppermute | solution.py:94
  147.4 4.2 %collective-permute-start.2 = (bf16[128,2048]{1,0:T(8,128)(2,1)S(1)}, bf16[128,2048]{1,0:T(8,128)(2,1)S(1)}, u32[]{:S(2)}, u32[]{:S(2)}) collective-permute-start(bf16[128,2048]{1,0:T(8,128)(2,1)S(1)} %get-tuple-element.19), channel_id=1, source_target_pairs={{0,6},{1,3},{2,0},{3,5},{4,2},{5,7},{6,4},{7,1},{8,14},{9,11},{10,... | collective-permute-start | bytes 1572872 | tf_op jit(solution)/shard_map/ppermute | solution.py:95
  151.6 0.0 collective-permute-done.1
  151.6 0.4 convert_add_fusion
  152.0 7.5 %collective-permute-done.3 = bf16[128,2048]{1,0:T(8,128)(2,1)S(1)} collective-permute-done((bf16[128,2048]{1,0:T(8,128)(2,1)S(1)}, bf16[128,2048]{1,0:T(8,128)(2,1)S(1)}, u32[]{:S(2)}, u32[]{:S(2)}) %collective-permute-start.3) | collective-permute-done | bytes 524320 | tf_op jit(solution)/shard_map/ppermute | solution.py:94
  159.5 0.1 fusion.6
  159.6 2.0 %collective-permute-start.4 = (bf16[128,2048]{1,0:T(8,128)(2,1)S(1)}, bf16[128,2048]{1,0:T(8,128)(2,1)S(1)}, u32[]{:S(2)}, u32[]{:S(2)}) collective-permute-start(bf16[128,2048]{1,0:T(8,128)(2,1)S(1)} %fusion.6), channel_id=1, source_target_pairs={{0,2},{1,7},{2,4},{3,1},{4,6},{5,3},{6,0},{7,5},{8,10},{9,15},{10,... | collective-permute-start | bytes 1572872 | tf_op jit(solution)/shard_map/ppermute | solution.py:100
  161.6 0.0 collective-permute-done.2
  161.6 9.2 %collective-permute-done.4 = bf16[128,2048]{1,0:T(8,128)(2,1)S(1)} collective-permute-done((bf16[128,2048]{1,0:T(8,128)(2,1)S(1)}, bf16[128,2048]{1,0:T(8,128)(2,1)S(1)}, u32[]{:S(2)}, u32[]{:S(2)}) %collective-permute-start.4) | collective-permute-done | bytes 524320 | tf_op jit(solution)/shard_map/ppermute | solution.py:100
  170.8 1.0 add_convert_fusion.1
  (4 shorter events, 0.1 us)
Async XLA Ops:
  111.7 3.1 %copy-start = (f32[2048]{0:T(1024)S(1)}, f32[2048]{0:T(1024)}, u32[]{:S(2)}) copy-start(f32[2048]{0:T(1024)} %param.12) | copy-start | bytes 24580
  111.8 3.1 %copy-start.1 = (f32[3,256]{1,0:T(4,128)S(1)}, f32[3,256]{1,0:T(4,128)}, u32[]{:S(2)}) copy-start(f32[3,256]{1,0:T(4,128)} %taps.1) | copy-start | bytes 9220
  123.4 18.3 %collective-permute-start = (bf16[256,2048]{1,0:T(8,128)(2,1)S(1)}, bf16[256,2048]{1,0:T(8,128)(2,1)S(1)}, u32[]{:S(2)}, u32[]{:S(2)}) collective-permute-start(bf16[256,2048]{1,0:T(8,128)(2,1)S(1)} %fusion.4), channel_id=1, source_target_pairs={{0,1},{1,0},{2,3},{3,2},{4,5},{5,4},{6,7},{7,6},{8,9},{9,8},{10,11... | collective-permute-start | bytes 3145736 | tf_op jit(solution)/shard_map/ppermute | solution.py:90
  142.1 9.5 %collective-permute-start.1 = (bf16[256,2048]{1,0:T(8,128)(2,1)S(1)}, bf16[256,2048]{1,0:T(8,128)(2,1)S(1)}, u32[]{:S(2)}, u32[]{:S(2)}) collective-permute-start(bf16[256,2048]{1,0:T(8,128)(2,1)S(1)} %fusion.5), channel_id=1, source_target_pairs={{0,1},{1,0},{2,3},{3,2},{4,5},{5,4},{6,7},{7,6},{8,9},{9,8},{10,11... | collective-permute-start | bytes 3145736 | tf_op jit(solution)/shard_map/ppermute | solution.py:96
  145.0 14.5 %collective-permute-start.3 = (bf16[128,2048]{1,0:T(8,128)(2,1)S(1)}, bf16[128,2048]{1,0:T(8,128)(2,1)S(1)}, u32[]{:S(2)}, u32[]{:S(2)}) collective-permute-start(bf16[128,2048]{1,0:T(8,128)(2,1)S(1)} %get-tuple-element.20), channel_id=1, source_target_pairs={{0,2},{1,7},{2,4},{3,1},{4,6},{5,3},{6,0},{7,5},{8,10},{9,15},{10,... | collective-permute-start | bytes 1572872 | tf_op jit(solution)/shard_map/ppermute | solution.py:94
  147.4 14.2 %collective-permute-start.2 = (bf16[128,2048]{1,0:T(8,128)(2,1)S(1)}, bf16[128,2048]{1,0:T(8,128)(2,1)S(1)}, u32[]{:S(2)}, u32[]{:S(2)}) collective-permute-start(bf16[128,2048]{1,0:T(8,128)(2,1)S(1)} %get-tuple-element.19), channel_id=1, source_target_pairs={{0,6},{1,3},{2,0},{3,5},{4,2},{5,7},{6,4},{7,1},{8,14},{9,11},{10,... | collective-permute-start | bytes 1572872 | tf_op jit(solution)/shard_map/ppermute | solution.py:95
  159.6 11.2 %collective-permute-start.4 = (bf16[128,2048]{1,0:T(8,128)(2,1)S(1)}, bf16[128,2048]{1,0:T(8,128)(2,1)S(1)}, u32[]{:S(2)}, u32[]{:S(2)}) collective-permute-start(bf16[128,2048]{1,0:T(8,128)(2,1)S(1)} %fusion.6), channel_id=1, source_target_pairs={{0,2},{1,7},{2,4},{3,1},{4,6},{5,3},{6,0},{7,5},{8,10},{9,15},{10,... | collective-permute-start | bytes 1572872 | tf_op jit(solution)/shard_map/ppermute | solution.py:100

commit v6 on v5

--- a/solution.py
+++ b/solution.py
@@ -10,7 +10,7 @@
 LIFT = 2.0**18
 LOW = 2.0**12
 LANES = 128
-PARTS = 2
+PARTS = 4
 ROWS = 512
 SUB = 128
 VMEM_BYTES = 32 * 2**20
@@ -107,20 +107,25 @@
 
     @pl.when(pl.program_id(0) == 0)
     def _():
-        fetch = pltpu.make_async_copy(far_piece, near_piece, ready)
-        fetch.start()
+        pltpu.make_async_copy(far_piece, near_piece, ready).start()
         carry[...] = jnp.zeros_like(carry)
         depth = weight.shape[0]
         rows = depth // near_piece.shape[0]
-        inputs, at = weight.shape[1] // LANES, 0
-        for piece in (*pieces, near_piece):
-            if piece is near_piece:
-                fetch.wait()
+        at = 0
+        for piece in pieces:
             for low in range(0, piece.shape[1], rows):
                 full = piece[:, low : low + rows, :].reshape(depth, LANES)
-                to, k = (weight, at) if at < inputs else (mixer, at - inputs)
-                to[:, k * LANES : (k + 1) * LANES] = full
+                weight[:, at * LANES : (at + 1) * LANES] = full
                 at += 1
+
+    @pl.when(pl.program_id(0) == pl.num_programs(0) - 1)
+    def _():
+        pltpu.make_async_copy(far_piece, near_piece, ready).wait()
+        depth = mixer.shape[0]
+        rows = depth // near_piece.shape[0]
+        for at in range(mixer.shape[1] // LANES):
+            full = near_piece[:, at * rows : (at + 1) * rows, :].reshape(depth, LANES)
+            mixer[:, at * LANES : (at + 1) * LANES] = full
 
     last = carry[...]
     row = lax.broadcasted_iota(jnp.int32, (8, width), 0)

time: 173 us -> 172 us (level)
  no operation moved by 1% of the time
where the time goes in v6:
time: 172 us; the launch traced here: 170 us
  blocking collectives  111 us (65%)
  starting transfers between devices  26.8 us (16%)
  waiting for transfers between devices  18.5 us (11%)
  Pallas kernels  7.65 us (4%)
  other arithmetic  3.87 us (2%)
  matrix products  1.89 us (1%)
    all_gather x1, blocking collectives, gathered(): pieces = lax.all_gather(packed.astype(jnp.float16), 'fs')  111 us
    ppermute x1, starting transfers between devices, summed_rows(): theirs = lax.ppermute(part(1 - core, (2, 3)), 'tp', swap)  16 us
    ppermute x1, waiting for transfers between devices, summed_rows(): ahead = lax.ppermute(onward, 'tp', toward(1))  9.2 us
    ppermute x1, waiting for transfers between devices, summed_rows(): carried = lax.ppermute(outward[:rows], 'tp', toward(1))  7.52 us
    pallas_call x1, Pallas kernels, gated_rows(): pl.pallas_call(gate_kernel, grid=(rows // ROWS,), in_specs=[pl.BlockSpec(...  6.59 us
    ppermute x1, starting transfers between devices, summed_rows(): behind = lax.ppermute(outward[rows:], 'tp', toward(-1))  4.21 us
  transfers between devices with their start and end apart: 5, of which 3 were waited for; matrix products, arithmetic and copies ran while one was open for 1% of the time, Pallas kernels for 0%

profile of v6, /device:TPU:39, one launch (start us, length us, event | category | flops | bytes accessed | tf_op | source)
XLA Modules:
  0.0 170.1 jit_solution(5179353422648328958)
XLA Ops:
  0.0 1.1 shard_map.109
  1.1 110.6 %all-gather.2 = f16[16640,128]{1,0:T(8,128)(2,1)S(1)} all-gather(f16[520,128]{1,0:T(8,128)(2,1)S(1)} %convert_element_type.85), channel_id=2, replica_groups=mesh['grp'=2,'fs'=32,'tp'=8] {'fs'}, dimensions={0}, use_global_device_ids=true | all-gather | bytes 4392960 | tf_op jit(solution)/shard_map/all_gather | solution.py:49
  111.7 0.0 copy-start
  111.8 0.0 copy-start.1
  111.8 2.2 %convert_convert_fusion = (bf16[32,128,128]{2,1,0:T(8,128)(2,1)}, bf16[32,128,128]{2,1,0:T(8,128)(2,1)S(1)}, bf16[32,128,128]{2,1,0:T(8,128)(2,1)S(1)}, bf16[32,128,128]{2,1,0:T(8,128)(2,1)S(1)}) fusion(f16[32,520,128]{2,1,0:T(8,128)(2,1)S(1)} %bitcast.10), kind=kLoop, calls=%fused_computation.12 | loop fusion | flops 4194304 | bytes 8388608 | tf_op jit(solution)/shard_map/convert_element_type | solution.py:59
  114.0 0.1 slice_multiply_fusion.3
  114.0 0.1 slice_multiply_fusion
  114.2 0.1 mul.139
  114.3 0.1 mul.137
  114.4 0.1 mul.135
  114.5 0.1 mul.147
  114.5 0.0 copy-done
  114.5 0.0 copy-done.1
  114.6 6.6 %shard_map.110 = (bf16[1024,256]{1,0:T(8,128)(2,1)S(1)}, bf16[2048,256]{1,0:T(8,128)(2,1)S(1)}) custom-call(bf16[1024,2048]{1,0:T(8,128)(2,1)} %tokens.1, f32[1,2048]{1,0:T(1,128)S(1)} %bitcast.8, f32[1,768]{1,0:T(1,128)S(1)} %reshape.31.columns, f32[3,256]{1,0:T(4,128)S(1)} %copy-done.1, bf16[32,128,128]{2,1,0:T(8,128)(2,1)S(1)} %get-tuple-element.13.refs_0_, ...), custom_call_target="tpu_custom_call" | custom-call | tf_op jit(solution)/shard_map/pallas_call | solution.py:161
  121.2 0.1 constant_dynamic-slice_fusion.1
  121.2 0.5 fusion.4
  121.7 16.0 %collective-permute-start = (bf16[256,2048]{1,0:T(8,128)(2,1)S(1)}, bf16[256,2048]{1,0:T(8,128)(2,1)S(1)}, u32[]{:S(2)}, u32[]{:S(2)}) collective-permute-start(bf16[256,2048]{1,0:T(8,128)(2,1)S(1)} %fusion.4), channel_id=1, source_target_pairs={{0,1},{1,0},{2,3},{3,2},{4,5},{5,4},{6,7},{7,6},{8,9},{9,8},{10,11... | collective-permute-start | bytes 3145736 | tf_op jit(solution)/shard_map/ppermute | solution.py:90
  137.7 0.5 fusion.5
  138.2 1.8 %collective-permute-done = bf16[256,2048]{1,0:T(8,128)(2,1)S(1)} collective-permute-done((bf16[256,2048]{1,0:T(8,128)(2,1)S(1)}, bf16[256,2048]{1,0:T(8,128)(2,1)S(1)}, u32[]{:S(2)}, u32[]{:S(2)}) %collective-permute-start) | collective-permute-done | bytes 1048608 | tf_op jit(solution)/shard_map/ppermute | solution.py:90
  140.0 0.5 add_convert_fusion
  140.5 2.3 %collective-permute-start.1 = (bf16[256,2048]{1,0:T(8,128)(2,1)S(1)}, bf16[256,2048]{1,0:T(8,128)(2,1)S(1)}, u32[]{:S(2)}, u32[]{:S(2)}) collective-permute-start(bf16[256,2048]{1,0:T(8,128)(2,1)S(1)} %fusion.5), channel_id=1, source_target_pairs={{0,1},{1,0},{2,3},{3,2},{4,5},{5,4},{6,7},{7,6},{8,9},{9,8},{10,11... | collective-permute-start | bytes 3145736 | tf_op jit(solution)/shard_map/ppermute | solution.py:96
  142.8 0.5 fusion.1
  143.3 0.1 fusion.26
  143.4 2.3 %collective-permute-start.3 = (bf16[128,2048]{1,0:T(8,128)(2,1)S(1)}, bf16[128,2048]{1,0:T(8,128)(2,1)S(1)}, u32[]{:S(2)}, u32[]{:S(2)}) collective-permute-start(bf16[128,2048]{1,0:T(8,128)(2,1)S(1)} %get-tuple-element.26), channel_id=1, source_target_pairs={{0,2},{1,7},{2,4},{3,1},{4,6},{5,3},{6,0},{7,5},{8,10},{9,15},{10,... | collective-permute-start | bytes 1572872 | tf_op jit(solution)/shard_map/ppermute | solution.py:94
  145.7 4.2 %collective-permute-start.2 = (bf16[128,2048]{1,0:T(8,128)(2,1)S(1)}, bf16[128,2048]{1,0:T(8,128)(2,1)S(1)}, u32[]{:S(2)}, u32[]{:S(2)}) collective-permute-start(bf16[128,2048]{1,0:T(8,128)(2,1)S(1)} %get-tuple-element.25), channel_id=1, source_target_pairs={{0,6},{1,3},{2,0},{3,5},{4,2},{5,7},{6,4},{7,1},{8,14},{9,11},{10,... | collective-permute-start | bytes 1572872 | tf_op jit(solution)/shard_map/ppermute | solution.py:95
  149.9 0.0 collective-permute-done.1
  149.9 0.4 convert_add_fusion
  150.3 7.5 %collective-permute-done.3 = bf16[128,2048]{1,0:T(8,128)(2,1)S(1)} collective-permute-done((bf16[128,2048]{1,0:T(8,128)(2,1)S(1)}, bf16[128,2048]{1,0:T(8,128)(2,1)S(1)}, u32[]{:S(2)}, u32[]{:S(2)}) %collective-permute-start.3) | collective-permute-done | bytes 524320 | tf_op jit(solution)/shard_map/ppermute | solution.py:94
  157.8 0.1 fusion.6
  157.9 2.0 %collective-permute-start.4 = (bf16[128,2048]{1,0:T(8,128)(2,1)S(1)}, bf16[128,2048]{1,0:T(8,128)(2,1)S(1)}, u32[]{:S(2)}, u32[]{:S(2)}) collective-permute-start(bf16[128,2048]{1,0:T(8,128)(2,1)S(1)} %fusion.6), channel_id=1, source_target_pairs={{0,2},{1,7},{2,4},{3,1},{4,6},{5,3},{6,0},{7,5},{8,10},{9,15},{10,... | collective-permute-start | bytes 1572872 | tf_op jit(solution)/shard_map/ppermute | solution.py:100
  159.9 0.0 collective-permute-done.2
  159.9 9.2 %collective-permute-done.4 = bf16[128,2048]{1,0:T(8,128)(2,1)S(1)} collective-permute-done((bf16[128,2048]{1,0:T(8,128)(2,1)S(1)}, bf16[128,2048]{1,0:T(8,128)(2,1)S(1)}, u32[]{:S(2)}, u32[]{:S(2)}) %collective-permute-start.4) | collective-permute-done | bytes 524320 | tf_op jit(solution)/shard_map/ppermute | solution.py:100
  169.1 1.0 add_convert_fusion.1
  (4 shorter events, 0.1 us)
Async XLA Ops:
  111.7 2.8 %copy-start = (f32[2048]{0:T(1024)S(1)}, f32[2048]{0:T(1024)}, u32[]{:S(2)}) copy-start(f32[2048]{0:T(1024)} %param.12) | copy-start | bytes 24580
  111.8 2.8 %copy-start.1 = (f32[3,256]{1,0:T(4,128)S(1)}, f32[3,256]{1,0:T(4,128)}, u32[]{:S(2)}) copy-start(f32[3,256]{1,0:T(4,128)} %taps.1) | copy-start | bytes 9220
  121.7 18.3 %collective-permute-start = (bf16[256,2048]{1,0:T(8,128)(2,1)S(1)}, bf16[256,2048]{1,0:T(8,128)(2,1)S(1)}, u32[]{:S(2)}, u32[]{:S(2)}) collective-permute-start(bf16[256,2048]{1,0:T(8,128)(2,1)S(1)} %fusion.4), channel_id=1, source_target_pairs={{0,1},{1,0},{2,3},{3,2},{4,5},{5,4},{6,7},{7,6},{8,9},{9,8},{10,11... | collective-permute-start | bytes 3145736 | tf_op jit(solution)/shard_map/ppermute | solution.py:90
  140.5 9.5 %collective-permute-start.1 = (bf16[256,2048]{1,0:T(8,128)(2,1)S(1)}, bf16[256,2048]{1,0:T(8,128)(2,1)S(1)}, u32[]{:S(2)}, u32[]{:S(2)}) collective-permute-start(bf16[256,2048]{1,0:T(8,128)(2,1)S(1)} %fusion.5), channel_id=1, source_target_pairs={{0,1},{1,0},{2,3},{3,2},{4,5},{5,4},{6,7},{7,6},{8,9},{9,8},{10,11... | collective-permute-start | bytes 3145736 | tf_op jit(solution)/shard_map/ppermute | solution.py:96
  143.4 14.5 %collective-permute-start.3 = (bf16[128,2048]{1,0:T(8,128)(2,1)S(1)}, bf16[128,2048]{1,0:T(8,128)(2,1)S(1)}, u32[]{:S(2)}, u32[]{:S(2)}) collective-permute-start(bf16[128,2048]{1,0:T(8,128)(2,1)S(1)} %get-tuple-element.26), channel_id=1, source_target_pairs={{0,2},{1,7},{2,4},{3,1},{4,6},{5,3},{6,0},{7,5},{8,10},{9,15},{10,... | collective-permute-start | bytes 1572872 | tf_op jit(solution)/shard_map/ppermute | solution.py:94
  145.7 14.2 %collective-permute-start.2 = (bf16[128,2048]{1,0:T(8,128)(2,1)S(1)}, bf16[128,2048]{1,0:T(8,128)(2,1)S(1)}, u32[]{:S(2)}, u32[]{:S(2)}) collective-permute-start(bf16[128,2048]{1,0:T(8,128)(2,1)S(1)} %get-tuple-element.25), channel_id=1, source_target_pairs={{0,6},{1,3},{2,0},{3,5},{4,2},{5,7},{6,4},{7,1},{8,14},{9,11},{10,... | collective-permute-start | bytes 1572872 | tf_op jit(solution)/shard_map/ppermute | solution.py:95
  157.9 11.2 %collective-permute-start.4 = (bf16[128,2048]{1,0:T(8,128)(2,1)S(1)}, bf16[128,2048]{1,0:T(8,128)(2,1)S(1)}, u32[]{:S(2)}, u32[]{:S(2)}) collective-permute-start(bf16[128,2048]{1,0:T(8,128)(2,1)S(1)} %fusion.6), channel_id=1, source_target_pairs={{0,2},{1,7},{2,4},{3,1},{4,6},{5,3},{6,0},{7,5},{8,10},{9,15},{10,... | collective-permute-start | bytes 1572872 | tf_op jit(solution)/shard_map/ppermute | solution.py:100
